TPU v7x, 32 devices: a whole 2x2x4 slice. The times are simulated.
32 devices in a mesh: rep: 2 (over y), fs: 4 (over z), tp: 4 (over x, core).
Axes of the slice: x: 2, y: 2, z: 4, core: 2. Of those that a mesh axis runs over, the one named last changes fastest.
Arguments:
- tokens: bfloat16 [4096, 2048], P(('rep', 'fs'), 'tp'), may hold values from -6 to 6
- outer_gate: float32 [2048, 512], P('fs', 'tp'), may hold values from -0.125 to 0.125
- inner_gate: float32 [2048, 512], P('fs', 'tp'), may hold values from -0.125 to 0.125
- mixer_value: float32 [2048, 512], P('fs', 'tp'), may hold values from -0.125 to 0.125
- mixer_scales: float32 [3, 512], P(None, 'tp'), may hold values from 0.5 to 2
- mixer_taps: float32 [3, 512], P(None, 'tp'), may hold values from -3.5 to 3.5
- mixer_out: float32 [512, 2048], P('fs', 'tp'), may hold values from -0.25 to 0.25
- out_scale: float32 [2048], P('tp'), may hold values from 0.3 to 3
- first_gain: float32 [2048], replicated, may hold values from 0.1 to 1.9
- first_shift: float32 [2048], replicated, may hold values from -2 to 2
- up_proj: float32 [2048, 3072], P('fs', 'tp'), may hold values from -0.125 to 0.125
- gate_proj: float32 [2048, 3072], P('fs', 'tp'), may hold values from -0.125 to 0.125
- up_scales: float32 [2, 3072], P(None, 'tp'), may hold values from 0.5 to 2
- ffn_taps: float32 [3, 2, 3072], P(None, None, 'tp'), may hold values from -3.5 to 3.5
- ffn_shift: float32 [2, 3072], P(None, 'tp'), may hold values from -3 to 3
- down_proj: float32 [3072, 2048], P('fs', 'tp'), may hold values from -0.109375 to 0.109375
- down_scale: float32 [2048], P('tp'), may hold values from 0.3 to 3
- second_gain: float32 [2048], replicated, may hold values from 0.1 to 1.9
- second_shift: float32 [2048], replicated, may hold values from -2 to 2
Outputs:
- layer_out: bfloat16 [4096, 2048], P(('rep', 'fs'), 'tp')
All inputs are finite; a program needn't handle non-finite values.
Results may differ from a plain program's by a relative error of at most 0.017.
Values may be sent and summed in bfloat16 or wider, within the bound.
A program may use at most 64 MiB of HBM per device.

v0:
```python
import functools

import jax
import jax.numpy as jnp
from jax import lax
from jax.experimental import pallas as pl
from jax.experimental.pallas import tpu as pltpu
from jax.sharding import PartitionSpec as P

LEN = 128


norm_eps = 1e-05
residual_weight = 8.0**0.25


def causal_mix(signal, kernel_taps):
    sequences = signal.reshape(-1, LEN, signal.shape[-1])
    padded = jnp.pad(sequences, ((0, 0), (2, 0), (0, 0)))
    mixed = (
        kernel_taps[0] * padded[:, :-2]
        + kernel_taps[1] * padded[:, 1:-1]
        + kernel_taps[2] * padded[:, 2:]
    )
    return mixed.reshape(signal.shape)


def lowered(matrix):
    return matrix.astype(jnp.bfloat16)


def single_fold(operand, portion):
    return jnp.dot(operand, portion, preferred_element_type=jnp.float32)


def fold_step(operand, pieces):
    result = []
    for number in range(len(pieces)):
        result.append(jnp.dot(operand, pieces[number], preferred_element_type=jnp.float32))
    return tuple(result)


def own_columns(vector, own_width):
    return lax.dynamic_slice_in_dim(vector, lax.axis_index("tp") * own_width, own_width, 0)


def scaled_norm(summed, average, spread, gain_vector, shift_vector):
    return (summed - average) * lax.rsqrt(spread + norm_eps) * gain_vector + shift_vector


def local(
    tokens,
    outer_gate,
    inner_gate,
    mixer_value,
    mixer_scales,
    mixer_taps,
    mixer_out,
    out_scale,
    first_gain,
    first_shift,
    up_proj,
    gate_proj,
    up_scales,
    ffn_taps,
    ffn_shift,
    down_proj,
    down_scale,
    second_gain,
    second_shift,
):
    own_width = tokens.shape[1]
    full_width = own_width * lax.axis_size("tp")
    token_whole = lax.all_gather(tokens, "tp", axis=1, tiled=True)
    outer_part, inner_part, value_part = fold_step(
        token_whole,
        (
            lax.all_gather(lowered(outer_gate), "fs", axis=0, tiled=True),
            lax.all_gather(lowered(inner_gate), "fs", axis=0, tiled=True),
            lax.all_gather(lowered(mixer_value), "fs", axis=0, tiled=True),
        ),
    )
    outer_part = (outer_part * mixer_scales[0]).astype(jnp.bfloat16)
    inner_part = (inner_part * mixer_scales[1]).astype(jnp.bfloat16)
    value_part = (value_part * mixer_scales[2]).astype(jnp.bfloat16)
    product = inner_part.astype(jnp.float32) * value_part.astype(jnp.float32)
    mixed_conv = (outer_part.astype(jnp.float32) * causal_mix(product, mixer_taps)).astype(
        jnp.bfloat16
    )
    conv_whole = lax.all_gather(mixed_conv, "tp", axis=1, tiled=True)
    mixer_sum = (
        single_fold(conv_whole, lax.all_gather(lowered(mixer_out), "fs", axis=0, tiled=True))
        * out_scale
    )
    first_sum = residual_weight * tokens.astype(jnp.float32) + mixer_sum
    row_total, row_square = lax.psum(
        (jnp.sum(first_sum, 1, keepdims=True), jnp.sum(first_sum * first_sum, 1, keepdims=True)),
        "tp",
    )
    average = row_total / full_width
    spread = row_square / full_width - average * average
    normed = scaled_norm(
        first_sum,
        average,
        spread,
        own_columns(first_gain, own_width),
        own_columns(first_shift, own_width),
    ).astype(jnp.bfloat16)
    normed_whole = lax.all_gather(normed, "tp", axis=1, tiled=True)
    up_matrix, gate_matrix = (
        lax.all_gather(lowered(up_proj), "fs", axis=0, tiled=True),
        lax.all_gather(lowered(gate_proj), "fs", axis=0, tiled=True),
    )
    up_linear = jnp.dot(normed_whole, up_matrix, preferred_element_type=jnp.float32)
    gate_linear = jnp.dot(normed_whole, gate_matrix, preferred_element_type=jnp.float32)
    up_linear = up_linear * up_scales[0]
    gate_linear = gate_linear * up_scales[1]
    up_mixed = causal_mix(up_linear, ffn_taps[:, 0]) + ffn_shift[0]
    gate_mixed = causal_mix(gate_linear, ffn_taps[:, 1]) + ffn_shift[1]
    hidden = (up_mixed * jax.nn.silu(gate_mixed)).astype(jnp.bfloat16)
    hidden_whole = lax.all_gather(hidden, "tp", axis=1, tiled=True)
    ffn_sum = (
        single_fold(hidden_whole, lax.all_gather(lowered(down_proj), "fs", axis=0, tiled=True))
        * down_scale
    )
    second_sum = residual_weight * normed.astype(jnp.float32) + ffn_sum
    second_total, second_square = lax.psum(
        (jnp.sum(second_sum, 1, keepdims=True), jnp.sum(second_sum * second_sum, 1, keepdims=True)),
        "tp",
    )
    second_average = second_total / full_width
    second_spread = second_square / full_width - second_average * second_average
    return scaled_norm(
        second_sum,
        second_average,
        second_spread,
        own_columns(second_gain, own_width),
        own_columns(second_shift, own_width),
    ).astype(jnp.bfloat16)


LANES = 128


def shifted_mix(signal, taps, first_tap):
    rows = lax.broadcasted_iota(jnp.int32, signal.shape, 0) % LEN
    one = jnp.where(rows >= 1, pltpu.roll(signal, 1, 0), 0.0)
    two = jnp.where(rows >= 2, pltpu.roll(signal, 2, 0), 0.0)
    return (
        taps[first_tap : first_tap + 1] * two
        + taps[first_tap + 1 : first_tap + 2] * one
        + taps[first_tap + 2 : first_tap + 3] * signal
    )


def dot32(left, right):
    return jnp.dot(left, right, preferred_element_type=jnp.float32)


def kernel(
    fs,
    tp,
    tokens_hbm,
    outer_hbm,
    inner_hbm,
    value_hbm,
    out_hbm,
    up_hbm,
    gate_hbm,
    down_hbm,
    narrow,
    model,
    wide,
    result,
    mix_f,
    out_f,
    up_f,
    gate_f,
    down_f,
    mix_g,
    out_g,
    ug_g,
    down_g,
    token_all,
    conv_all,
    norm_all,
    hidden_all,
    first_sum,
    total,
    stats,
    load_sem,
    send_z,
    send_y,
    recv_z,
    recv_y,
    send_x,
    recv_x,
    send_s,
    recv_s,
):
    r, z, t = lax.axis_index("rep"), lax.axis_index("fs"), lax.axis_index("tp")
    sibling = t + 1 - 2 * (t % 2)
    across = (t + 2) % tp
    diagonal = (sibling + 2) % tp
    other = 1 - r
    rows, own_width = result.shape
    full_width = own_width * tp
    channels = conv_all.shape[2]
    blocks = ug_g.shape[1]

    sources = (tokens_hbm, outer_hbm, inner_hbm, value_hbm, out_hbm, up_hbm, gate_hbm, down_hbm)
    places = (token_all.at[t], mix_f.at[0], mix_f.at[1], mix_f.at[2], out_f, up_f, gate_f, down_f)
    loads = [
        pltpu.make_async_copy(source, place, load_sem.at[number])
        for number, (source, place) in enumerate(zip(sources, places))
    ]
    for load in loads:
        load.start()

    barrier = pltpu.get_barrier_semaphore()
    for peer in (sibling, across, diagonal):
        pl.semaphore_signal(barrier, inc=1, device_id={"tp": peer}, device_id_type=pl.DeviceIdType.MESH)
    pl.semaphore_signal(barrier, inc=1, device_id={"rep": other}, device_id_type=pl.DeviceIdType.MESH)

    @pl.when(z > 0)
    def _():
        pl.semaphore_signal(barrier, inc=1, device_id={"fs": z - 1}, device_id_type=pl.DeviceIdType.MESH)

    @pl.when(z < fs - 1)
    def _():
        pl.semaphore_signal(barrier, inc=1, device_id={"fs": z + 1}, device_id_type=pl.DeviceIdType.MESH)

    inside = (z > 0) & (z < fs - 1)

    @pl.when(inside)
    def _():
        pl.semaphore_wait(barrier, 6)

    @pl.when(jnp.logical_not(inside))
    def _():
        pl.semaphore_wait(barrier, 5)

    def hop(number, slot, ref, peer, kind):
        return pltpu.make_async_remote_copy(
            src_ref=ref(slot),
            dst_ref=ref(slot),
            send_sem=send_x.at[number, kind],
            recv_sem=recv_x.at[number, slot],
            device_id={"tp": peer},
            device_id_type=pl.DeviceIdType.MESH,
        )

    def exchange_start(number, ref):
        hop(number, t, ref, across, 0).start()
        hop(number, t, ref, sibling, 1).start()

    def exchange_pass(number, ref):
        hop(number, across, ref, across, 0).wait_recv()
        hop(number, across, ref, sibling, 2).start()

    def exchange_end(number, ref):
        hop(number, sibling, ref, sibling, 1).wait_recv()
        hop(number, diagonal, ref, sibling, 2).wait_recv()

    def exchange_sent(number, ref):
        hop(number, t, ref, across, 0).wait_send()
        hop(number, t, ref, sibling, 1).wait_send()
        hop(number, across, ref, sibling, 2).wait_send()

    def token_block(slot):
        return token_all.at[slot]

    def conv_block(slot):
        return conv_all.at[slot]

    def norm_block(slot):
        return norm_all.at[slot]

    def hidden_block(number):
        return lambda slot: hidden_all.at[slot, number]

    def mix_unit(part):
        size = mix_g.shape[1] // 4
        return lambda source, half: mix_g.at[source, pl.ds(pl.multiple_of((part * 2 + half) * size, size), size)]

    def out_unit(source, half):
        size = out_g.shape[1] // 2
        return out_g.at[source, pl.ds(pl.multiple_of(half * size, size), size)]

    def ug_unit(block):
        size = ug_g.shape[2] // 2
        return lambda source, half: ug_g.at[source, block, pl.ds(pl.multiple_of(half * size, size), size)]

    def down_unit(part):
        size = LANES
        return lambda source, half: down_g.at[source, pl.ds(pl.multiple_of((part * 2 + half) * size, size), size)]

    units = [mix_unit(0), mix_unit(1), out_unit]
    units += [ug_unit(block) for block in range(blocks)]
    units += [down_unit(part) for part in range(blocks // 2)]
    count = len(units)
    first_ug, first_down = 3, 3 + blocks

    def along(unit, source, target, way):
        ref = units[unit](source, r)
        return pltpu.make_async_remote_copy(
            src_ref=ref,
            dst_ref=ref,
            send_sem=send_z.at[unit, source, way],
            recv_sem=recv_z.at[unit, source],
            device_id={"fs": target},
            device_id_type=pl.DeviceIdType.MESH,
        )

    def over(unit, source, half):
        ref = units[unit](source, half)
        return pltpu.make_async_remote_copy(
            src_ref=ref,
            dst_ref=ref,
            send_sem=send_y.at[unit, source],
            recv_sem=recv_y.at[unit, source],
            device_id={"rep": other},
            device_id_type=pl.DeviceIdType.MESH,
        )

    def own(unit):
        @pl.when(z < fs - 1)
        def _():
            along(unit, z, z + 1, 0).start()

        @pl.when(z > 0)
        def _():
            along(unit, z, z - 1, 1).start()

    def own_sent(unit):
        @pl.when(z < fs - 1)
        def _():
            along(unit, z, z + 1, 0).wait_send()

        @pl.when(z > 0)
        def _():
            along(unit, z, z - 1, 1).wait_send()

    def passed(unit, distance, sent):
        @pl.when(z >= distance)
        def _():
            source = z - distance
            if not sent:
                along(unit, source, z, 0).wait_recv()

            @pl.when(z < fs - 1)
            def _():
                copy = along(unit, source, z + 1, 0)
                copy.wait_send() if sent else copy.start()

            copy = over(unit, source, r)
            copy.wait_send() if sent else copy.start()

        @pl.when(z + distance < fs)
        def _():
            source = z + distance
            if not sent:
                along(unit, source, z, 1).wait_recv()

            @pl.when(z > 0)
            def _():
                copy = along(unit, source, z - 1, 1)
                copy.wait_send() if sent else copy.start()

            copy = over(unit, source, r)
            copy.wait_send() if sent else copy.start()

    def step(number):
        if number < count:
            own(number)
        for distance in range(1, fs):
            if 0 <= number - distance < count:
                passed(number - distance, distance, False)

    def need(unit):
        for source in range(fs):

            @pl.when(z != source)
            def _():
                over(unit, source, other).wait_recv()

    def lower_block(block):
        columns = slice(block * LANES, (block + 1) * LANES)
        ug_g[z, block, :, :LANES] = up_f[:, columns].astype(jnp.bfloat16)
        ug_g[z, block, :, LANES:] = gate_f[:, columns].astype(jnp.bfloat16)

    def summing(number, peer, slot, kind):
        return pltpu.make_async_remote_copy(
            src_ref=stats.at[number, slot],
            dst_ref=stats.at[number, slot],
            send_sem=send_s.at[number, kind],
            recv_sem=recv_s.at[number, slot],
            device_id={"tp": peer},
            device_id_type=pl.DeviceIdType.MESH,
        )

    def sums_start(number, summed):
        lane = lax.broadcasted_iota(jnp.int32, (rows, LANES), 1)
        one = jnp.sum(summed, axis=1, keepdims=True)
        two = jnp.sum(summed * summed, axis=1, keepdims=True)
        stats[number, t] = jnp.transpose(jnp.where(lane == 0, one, two))[:8]
        for kind, peer in enumerate((across, diagonal, sibling)):
            summing(number, peer, t, kind).start()

    def sums_end(number):
        for kind, peer in enumerate((across, diagonal, sibling)):
            summing(number, peer, peer, kind).wait_recv()
        whole = stats[number, 0]
        for slot in range(1, tp):
            whole = whole + stats[number, slot]
        back = jnp.transpose(jnp.concatenate([whole] * (LANES // 8), axis=0))
        average = back[:, 0:1] / full_width
        return average, back[:, 1:2] / full_width - average * average

    def mixer():
        for unit in (0, 1):
            need(unit)
        exchange_end(0, token_block)
        parts = dot32(token_all[0], mix_g[0])
        for slot in range(1, tp):
            parts = parts + dot32(token_all[slot], mix_g[slot])
        scaled = [
            (parts[:, part * channels : (part + 1) * channels] * narrow[part : part + 1])
            .astype(jnp.bfloat16)
            .astype(jnp.float32)
            for part in range(3)
        ]
        mixed = scaled[0] * shifted_mix(scaled[1] * scaled[2], narrow, 3)
        conv_all[t] = mixed.astype(jnp.bfloat16)
        exchange_start(1, conv_block)

    def mixer_output():
        need(2)
        exchange_end(1, conv_block)
        summed = dot32(conv_all[0], out_g[0])
        for slot in range(1, tp):
            summed = summed + dot32(conv_all[slot], out_g[slot])
        summed = summed * model[0:1] + residual_weight * token_all[t].astype(jnp.float32)
        first_sum[...] = summed
        sums_start(0, summed)

    def first_norm():
        average, spread = sums_end(0)
        norm_all[t] = scaled_norm(first_sum[...], average, spread, model[1:2], model[2:3]).astype(jnp.bfloat16)
        exchange_start(2, norm_block)

    def hidden(block):
        need(first_ug + block)
        both = dot32(norm_all[0], ug_g[0, block])
        for slot in range(1, tp):
            both = both + dot32(norm_all[slot], ug_g[slot, block])
        taps = wide[:, block * LANES : (block + 1) * LANES]
        up_mixed = shifted_mix(both[:, :LANES] * taps[0:1], taps, 2) + taps[8:9]
        gate_mixed = shifted_mix(both[:, LANES:] * taps[1:2], taps, 5) + taps[9:10]
        hidden_all[t, block] = (up_mixed * gate_mixed / (1.0 + jnp.exp(-gate_mixed))).astype(jnp.bfloat16)
        exchange_start(3 + block, hidden_block(block))

    def down(part):
        need(first_down + part)
        for block in (2 * part, 2 * part + 1):
            exchange_end(3 + block, hidden_block(block))
        summed = None
        for slot in range(tp):
            left = jnp.concatenate([hidden_all[slot, 2 * part], hidden_all[slot, 2 * part + 1]], axis=1)
            term = dot32(left, down_g[slot, part * 2 * LANES : (part + 1) * 2 * LANES])
            summed = term if summed is None else summed + term
        total[...] = summed if part == 0 else total[...] + summed

    for load in loads[:4]:
        load.wait()
    exchange_start(0, token_block)
    for part in range(3):
        mix_g[z, :, part * channels : (part + 1) * channels] = mix_f[part].astype(jnp.bfloat16)
    step(0)
    step(1)
    loads[4].wait()
    out_g[z] = out_f[...].astype(jnp.bfloat16)
    step(2)
    exchange_pass(0, token_block)
    loads[5].wait()
    loads[6].wait()
    loads[7].wait()
    lower_block(0)
    step(3)
    lower_block(1)
    step(4)
    mixer()
    lower_block(2)
    step(5)
    exchange_pass(1, conv_block)
    mixer_output()
    lower_block(3)
    step(6)
    first_norm()
    lower_block(4)
    step(7)
    for block in range(5, blocks):
        lower_block(block)
    exchange_pass(2, norm_block)
    step(8)
    down_g[z] = down_f[...].astype(jnp.bfloat16)
    exchange_end(2, norm_block)
    hidden(0)
    number = 9
    ready = 1
    moved = 0
    while ready < blocks:
        step(number)
        number += 1
        while moved < ready:
            exchange_pass(3 + moved, hidden_block(moved))
            moved += 1
        while ready < blocks and first_ug + ready + fs - 1 <= number - 1:
            hidden(ready)
            ready += 1
    for part in range(blocks // 2):
        while number <= first_down + part + fs - 1:
            step(number)
            number += 1
        while moved < blocks:
            exchange_pass(3 + moved, hidden_block(moved))
            moved += 1
        down(part)

    second = total[...] * model[3:4] + residual_weight * norm_all[t].astype(jnp.float32)
    total[...] = second
    sums_start(1, second)

    for unit in range(count):
        own_sent(unit)
        for distance in range(1, fs):
            passed(unit, distance, True)
    refs = [token_block, conv_block, norm_block] + [hidden_block(block) for block in range(blocks)]
    for place, ref in enumerate(refs):
        exchange_sent(place, ref)
    average, spread = sums_end(1)
    result[...] = scaled_norm(total[...], average, spread, model[4:5], model[5:6]).astype(result.dtype)
    for place in range(2):
        for kind, peer in enumerate((across, diagonal, sibling)):
            summing(place, peer, t, kind).wait_send()


def fused(
    fs,
    tp,
    tokens,
    outer_gate,
    inner_gate,
    mixer_value,
    mixer_scales,
    mixer_taps,
    mixer_out,
    out_scale,
    first_gain,
    first_shift,
    up_proj,
    gate_proj,
    up_scales,
    ffn_taps,
    ffn_shift,
    down_proj,
    down_scale,
    second_gain,
    second_shift,
):
    rows, own_width = tokens.shape
    depth, channels = outer_gate.shape
    hidden = up_proj.shape[1]
    blocks = hidden // LANES
    count = 3 + blocks + blocks // 2
    narrow = jnp.concatenate([mixer_scales, mixer_taps], axis=0)
    model = jnp.stack(
        [
            out_scale,
            own_columns(first_gain, own_width),
            own_columns(first_shift, own_width),
            down_scale,
            own_columns(second_gain, own_width),
            own_columns(second_shift, own_width),
        ]
    )
    wide = jnp.concatenate([up_scales, ffn_taps[:, 0], ffn_taps[:, 1], ffn_shift], axis=0)
    any_space = pl.BlockSpec(memory_space=pl.ANY)
    in_vmem = pl.BlockSpec(memory_space=pltpu.VMEM)
    return pl.pallas_call(
        functools.partial(kernel, fs, tp),
        out_shape=jax.ShapeDtypeStruct((rows, own_width), jnp.bfloat16),
        in_specs=[any_space] * 8 + [in_vmem] * 3,
        out_specs=in_vmem,
        scratch_shapes=[
            pltpu.VMEM((3, depth, channels), jnp.float32),
            pltpu.VMEM(mixer_out.shape, jnp.float32),
            pltpu.VMEM(up_proj.shape, jnp.float32),
            pltpu.VMEM(gate_proj.shape, jnp.float32),
            pltpu.VMEM(down_proj.shape, jnp.float32),
            pltpu.VMEM((fs, depth, 3 * channels), jnp.bfloat16),
            pltpu.VMEM((fs,) + mixer_out.shape, jnp.bfloat16),
            pltpu.VMEM((fs, blocks, depth, 2 * LANES), jnp.bfloat16),
            pltpu.VMEM((fs,) + down_proj.shape, jnp.bfloat16),
            pltpu.VMEM((tp, rows, own_width), jnp.bfloat16),
            pltpu.VMEM((tp, rows, channels), jnp.bfloat16),
            pltpu.VMEM((tp, rows, own_width), jnp.bfloat16),
            pltpu.VMEM((tp, blocks, rows, LANES), jnp.bfloat16),
            pltpu.VMEM((rows, own_width), jnp.float32),
            pltpu.VMEM((rows, own_width), jnp.float32),
            pltpu.VMEM((2, tp, 8, rows), jnp.float32),
            pltpu.SemaphoreType.DMA((8,)),
            pltpu.SemaphoreType.DMA((count, fs, 2)),
            pltpu.SemaphoreType.DMA((count, fs)),
            pltpu.SemaphoreType.DMA((count, fs)),
            pltpu.SemaphoreType.DMA((count, fs)),
            pltpu.SemaphoreType.DMA((3 + blocks, 3)),
            pltpu.SemaphoreType.DMA((3 + blocks, tp)),
            pltpu.SemaphoreType.DMA((2, 3)),
            pltpu.SemaphoreType.DMA((2, tp)),
        ],
        compiler_params=pltpu.CompilerParams(
            collective_id=0, has_side_effects=True, vmem_limit_bytes=60 * 1024 * 1024
        ),
    )(
        tokens,
        outer_gate,
        inner_gate,
        mixer_value,
        mixer_out,
        up_proj,
        gate_proj,
        down_proj,
        narrow,
        model,
        wide,
    )


def fits(mesh):
    return mesh.shape["rep"] == 2 and mesh.shape["fs"] == 4 and mesh.shape["tp"] == 4


def solution(mesh):
    body = functools.partial(fused, mesh.shape["fs"], mesh.shape["tp"]) if fits(mesh) else local
    return jax.shard_map(
        body,
        mesh=mesh,
        in_specs=(
            P(("rep", "fs"), "tp"),
            P("fs", "tp"),
            P("fs", "tp"),
            P("fs", "tp"),
            P(None, "tp"),
            P(None, "tp"),
            P("fs", "tp"),
            P("tp"),
            P(),
            P(),
            P("fs", "tp"),
            P("fs", "tp"),
            P(None, "tp"),
            P(None, None, "tp"),
            P(None, "tp"),
            P("fs", "tp"),
            P("tp"),
            P(),
            P(),
        ),
        out_specs=P(("rep", "fs"), "tp"),
        check_vma=False,
    )
```

profile of v0, /device:TPU:0, one launch (start us, length us, event | category | flops | bytes accessed | tf_op | source)
XLA Modules:
  0.0 134.8 jit_solution(2091710055497902113)
XLA Ops:
  0.0 0.8 dynamic_slice.12
  0.8 0.8 dynamic_slice.13
  1.5 0.8 dynamic_slice.14
  2.3 0.8 dynamic_slice.15
  3.0 1.3 pad_maximum_fusion.1.narrow
  4.3 1.3 stack.27.model
  5.7 0.8 fusion
  6.5 1.3 %pad_maximum_fusion.wide = f32[10,768]{1,0:T(8,128)} fusion(f32[2,768]{1,0:T(2,128)} %param.33, f32[3,768]{1,0:T(4,128)S(1)} %get-tuple-element.7, f32[3,768]{1,0:T(4,128)S(1)} %get-tuple-element.8, f32[2,768]{1,0:T(2,128)} %param.31), kind=kLoop, calls=%fused_computation | loop fusion | flops 23040 | bytes 61440 | tf_op jit(solution)/shard_map/concatenate | solution.py:587
  7.8 125.1 %shard_map.181 = bf16[512,512]{1,0:T(8,128)(2,1)} custom-call(bf16[512,512]{1,0:T(8,128)(2,1)} %tokens_hbm.1, f32[512,128]{1,0:T(8,128)} %outer_hbm.1, f32[512,128]{1,0:T(8,128)} %inner_hbm.1, f32[512,128]{1,0:T(8,128)} %value_hbm.1, f32[128,512]{1,0:T(8,128)} %out_hbm.1, f32[512,768]{1,0:T(8,128)} %up_hbm.1, f32[512,768]{1,0:T(8,128)} %gate_hbm.1, ...), custom_call_target="tpu_custom_call" | custom-call | tf_op jit(solution)/shard_map/pallas_call | solution.py:590
  132.9 1.9 %copy.27 = bf16[512,512]{1,0:T(8,128)(2,1)} copy(bf16[512,512]{1,0:T(8,128)(2,1)} %shard_map.181) | data formatting | bytes 1048576
  (1 shorter events, 0.0 us)
where the time goes:
time: 135 us
  Pallas kernels  125 us (93%)
  local copies, waits for them, and re-layouts  7.05 us (5%)
  other arithmetic  2.64 us (2%)
    pallas_call x1, Pallas kernels, fused(): pl.pallas_call(functools.partial(kernel, fs, tp), out_shape=jax.ShapeDtyp...  125 us
    dynamic_slice x4, local copies, waits for them, and re-layouts, own_columns(): lax.dynamic_slice_in_dim(vector, lax.axis_index('tp') * own_width, own_wi...  3.04 us

commit v1 on v0

v1 whole, which is shorter than its diff:
```python
import functools

import jax
import jax.numpy as jnp
from jax import lax
from jax.experimental import pallas as pl
from jax.experimental.pallas import tpu as pltpu
from jax.sharding import PartitionSpec as P

LEN = 128


norm_eps = 1e-05
residual_weight = 8.0**0.25


def causal_mix(signal, kernel_taps):
    sequences = signal.reshape(-1, LEN, signal.shape[-1])
    padded = jnp.pad(sequences, ((0, 0), (2, 0), (0, 0)))
    mixed = (
        kernel_taps[0] * padded[:, :-2]
        + kernel_taps[1] * padded[:, 1:-1]
        + kernel_taps[2] * padded[:, 2:]
    )
    return mixed.reshape(signal.shape)


def lowered(matrix):
    return matrix.astype(jnp.bfloat16)


def single_fold(operand, portion):
    return jnp.dot(operand, portion, preferred_element_type=jnp.float32)


def fold_step(operand, pieces):
    result = []
    for number in range(len(pieces)):
        result.append(jnp.dot(operand, pieces[number], preferred_element_type=jnp.float32))
    return tuple(result)


def own_columns(vector, own_width):
    return lax.dynamic_slice_in_dim(vector, lax.axis_index("tp") * own_width, own_width, 0)


def scaled_norm(summed, average, spread, gain_vector, shift_vector):
    return (summed - average) * lax.rsqrt(spread + norm_eps) * gain_vector + shift_vector


def local(
    tokens,
    outer_gate,
    inner_gate,
    mixer_value,
    mixer_scales,
    mixer_taps,
    mixer_out,
    out_scale,
    first_gain,
    first_shift,
    up_proj,
    gate_proj,
    up_scales,
    ffn_taps,
    ffn_shift,
    down_proj,
    down_scale,
    second_gain,
    second_shift,
):
    own_width = tokens.shape[1]
    full_width = own_width * lax.axis_size("tp")
    token_whole = lax.all_gather(tokens, "tp", axis=1, tiled=True)
    outer_part, inner_part, value_part = fold_step(
        token_whole,
        (
            lax.all_gather(lowered(outer_gate), "fs", axis=0, tiled=True),
            lax.all_gather(lowered(inner_gate), "fs", axis=0, tiled=True),
            lax.all_gather(lowered(mixer_value), "fs", axis=0, tiled=True),
        ),
    )
    outer_part = (outer_part * mixer_scales[0]).astype(jnp.bfloat16)
    inner_part = (inner_part * mixer_scales[1]).astype(jnp.bfloat16)
    value_part = (value_part * mixer_scales[2]).astype(jnp.bfloat16)
    product = inner_part.astype(jnp.float32) * value_part.astype(jnp.float32)
    mixed_conv = (outer_part.astype(jnp.float32) * causal_mix(product, mixer_taps)).astype(
        jnp.bfloat16
    )
    conv_whole = lax.all_gather(mixed_conv, "tp", axis=1, tiled=True)
    mixer_sum = (
        single_fold(conv_whole, lax.all_gather(lowered(mixer_out), "fs", axis=0, tiled=True))
        * out_scale
    )
    first_sum = residual_weight * tokens.astype(jnp.float32) + mixer_sum
    row_total, row_square = lax.psum(
        (jnp.sum(first_sum, 1, keepdims=True), jnp.sum(first_sum * first_sum, 1, keepdims=True)),
        "tp",
    )
    average = row_total / full_width
    spread = row_square / full_width - average * average
    normed = scaled_norm(
        first_sum,
        average,
        spread,
        own_columns(first_gain, own_width),
        own_columns(first_shift, own_width),
    ).astype(jnp.bfloat16)
    normed_whole = lax.all_gather(normed, "tp", axis=1, tiled=True)
    up_matrix, gate_matrix = (
        lax.all_gather(lowered(up_proj), "fs", axis=0, tiled=True),
        lax.all_gather(lowered(gate_proj), "fs", axis=0, tiled=True),
    )
    up_linear = jnp.dot(normed_whole, up_matrix, preferred_element_type=jnp.float32)
    gate_linear = jnp.dot(normed_whole, gate_matrix, preferred_element_type=jnp.float32)
    up_linear = up_linear * up_scales[0]
    gate_linear = gate_linear * up_scales[1]
    up_mixed = causal_mix(up_linear, ffn_taps[:, 0]) + ffn_shift[0]
    gate_mixed = causal_mix(gate_linear, ffn_taps[:, 1]) + ffn_shift[1]
    hidden = (up_mixed * jax.nn.silu(gate_mixed)).astype(jnp.bfloat16)
    hidden_whole = lax.all_gather(hidden, "tp", axis=1, tiled=True)
    ffn_sum = (
        single_fold(hidden_whole, lax.all_gather(lowered(down_proj), "fs", axis=0, tiled=True))
        * down_scale
    )
    second_sum = residual_weight * normed.astype(jnp.float32) + ffn_sum
    second_total, second_square = lax.psum(
        (jnp.sum(second_sum, 1, keepdims=True), jnp.sum(second_sum * second_sum, 1, keepdims=True)),
        "tp",
    )
    second_average = second_total / full_width
    second_spread = second_square / full_width - second_average * second_average
    return scaled_norm(
        second_sum,
        second_average,
        second_spread,
        own_columns(second_gain, own_width),
        own_columns(second_shift, own_width),
    ).astype(jnp.bfloat16)


LANES = 128
GUEST_PARTS = 2


def shifted_mix(signal, first, second, third):
    rows = lax.broadcasted_iota(jnp.int32, signal.shape, 0) % LEN
    one = jnp.where(rows >= 1, pltpu.roll(signal, 1, 0), 0.0)
    two = jnp.where(rows >= 2, pltpu.roll(signal, 2, 0), 0.0)
    return first * two + second * one + third * signal


def dot32(left, right):
    return jnp.dot(left, right, preferred_element_type=jnp.float32)


def kernel(
    fs,
    tp,
    tokens_hbm,
    outer_hbm,
    inner_hbm,
    value_hbm,
    out_hbm,
    up_hbm,
    gate_hbm,
    down_hbm,
    mixer_scales,
    mixer_taps,
    out_scale,
    first_gain,
    first_shift,
    up_scales,
    ffn_taps,
    ffn_shift,
    down_scale,
    second_gain,
    second_shift,
    result,
    mix_f,
    out_f,
    up_f,
    gate_f,
    down_f,
    mix_g,
    out_g,
    ug_g,
    down_g,
    token_all,
    conv_all,
    norm_all,
    guest_all,
    hidden_all,
    hidden_out,
    first_sum,
    total,
    stats,
    load_sem,
    send_z,
    send_y,
    recv_z,
    recv_y,
    send_x,
    recv_x,
    send_s,
    recv_s,
    send_g,
    recv_g,
    send_h,
    recv_h,
):
    r, z, t = lax.axis_index("rep"), lax.axis_index("fs"), lax.axis_index("tp")
    sibling = t + 1 - 2 * (t % 2)
    across = (t + 2) % tp
    diagonal = (sibling + 2) % tp
    other = 1 - r
    rows, own_width = result.shape
    full_width = own_width * tp
    channels = conv_all.shape[2]
    blocks = ug_g.shape[1]
    last = fs - 1
    own_lanes = pl.ds(pl.multiple_of(t * own_width, own_width), own_width)

    sources = (tokens_hbm, outer_hbm, inner_hbm, value_hbm, out_hbm, up_hbm, gate_hbm, down_hbm)
    places = (token_all.at[t], mix_f.at[0], mix_f.at[1], mix_f.at[2], out_f, up_f, gate_f, down_f)
    loads = [
        pltpu.make_async_copy(source, place, load_sem.at[number])
        for number, (source, place) in enumerate(zip(sources, places))
    ]
    for load in loads:
        load.start()

    barrier = pltpu.get_barrier_semaphore()
    for peer in (sibling, across, diagonal):
        pl.semaphore_signal(barrier, inc=1, device_id={"tp": peer}, device_id_type=pl.DeviceIdType.MESH)
    pl.semaphore_signal(barrier, inc=1, device_id={"rep": other}, device_id_type=pl.DeviceIdType.MESH)

    @pl.when(z > 0)
    def _():
        pl.semaphore_signal(barrier, inc=1, device_id={"fs": z - 1}, device_id_type=pl.DeviceIdType.MESH)

    @pl.when(z < last)
    def _():
        pl.semaphore_signal(barrier, inc=1, device_id={"fs": z + 1}, device_id_type=pl.DeviceIdType.MESH)

    inside = (z > 0) & (z < last)

    @pl.when(inside)
    def _():
        pl.semaphore_wait(barrier, 6)

    @pl.when(jnp.logical_not(inside))
    def _():
        pl.semaphore_wait(barrier, 5)

    def hop(number, slot, ref, peer, kind):
        return pltpu.make_async_remote_copy(
            src_ref=ref(slot),
            dst_ref=ref(slot),
            send_sem=send_x.at[number, kind],
            recv_sem=recv_x.at[number, slot],
            device_id={"tp": peer},
            device_id_type=pl.DeviceIdType.MESH,
        )

    def token_block(slot):
        return token_all.at[slot]

    def conv_block(slot):
        return conv_all.at[slot]

    def norm_block(slot):
        return norm_all.at[slot]

    def hidden_block(number):
        return lambda slot: hidden_all.at[slot, number]

    guest_rows = rows // GUEST_PARTS

    def guest_block(part):
        return lambda slot: guest_all.at[slot, pl.ds(part * guest_rows, guest_rows)]

    exchanges = [token_block, conv_block, norm_block]
    exchanges += [hidden_block(block) for block in range(blocks)]
    exchanges += [guest_block(part) for part in range(GUEST_PARTS)]
    first_hidden, first_guest = 3, 3 + blocks

    def mix_unit(part):
        size = mix_g.shape[1] // 4
        return lambda source, half: mix_g.at[source, pl.ds(pl.multiple_of((part * 2 + half) * size, size), size)]

    def out_unit(source, half):
        size = out_g.shape[1] // 2
        return out_g.at[source, pl.ds(pl.multiple_of(half * size, size), size)]

    def ug_unit(block):
        size = ug_g.shape[2] // 2
        return lambda source, half: ug_g.at[source, block, pl.ds(pl.multiple_of(half * size, size), size)]

    def down_unit(part):
        size = LANES
        return lambda source, half: down_g.at[source, pl.ds(pl.multiple_of((part * 2 + half) * size, size), size)]

    parts = blocks // 2
    units = [mix_unit(0), mix_unit(1), out_unit]
    units += [down_unit(part) for part in range(parts)]
    units += [ug_unit(block) for block in range(blocks)]
    count = len(units)
    first_down, first_ug = 3, 3 + parts
    whole = [True] * 3 + [False] * (parts - 1) + [True] + [True] * blocks

    def summing(number, peer, slot, kind):
        return pltpu.make_async_remote_copy(
            src_ref=stats.at[number, slot],
            dst_ref=stats.at[number, slot],
            send_sem=send_s.at[number, kind],
            recv_sem=recv_s.at[number, slot],
            device_id={"tp": peer},
            device_id_type=pl.DeviceIdType.MESH,
        )

    def program(middle):
        if middle:
            outer, inner, far = (z - 1) * last, last - z, (2 - z) * last
        else:
            near = 1 + z // last
            beyond, far = last - near, last - z
        sent = []

        def begin(copy):
            copy.start()
            sent.append(copy)

        def exchange_start(number):
            begin(hop(number, t, exchanges[number], across, 0))
            begin(hop(number, t, exchanges[number], sibling, 1))

        def exchange_pass(number):
            hop(number, across, exchanges[number], across, 0).wait_recv()
            begin(hop(number, across, exchanges[number], sibling, 2))

        def exchange_end(number):
            hop(number, sibling, exchanges[number], sibling, 1).wait_recv()
            hop(number, diagonal, exchanges[number], sibling, 2).wait_recv()

        def along(unit, source, target, way, kind):
            ref = units[unit](source, other if kind else r)
            return pltpu.make_async_remote_copy(
                src_ref=ref,
                dst_ref=ref,
                send_sem=send_z.at[unit, source, way, kind],
                recv_sem=recv_z.at[unit, source, kind],
                device_id={"fs": target},
                device_id_type=pl.DeviceIdType.MESH,
            )

        def over(unit, source, half):
            ref = units[unit](source, half)
            return pltpu.make_async_remote_copy(
                src_ref=ref,
                dst_ref=ref,
                send_sem=send_y.at[unit, source],
                recv_sem=recv_y.at[unit, source],
                device_id={"rep": other},
                device_id_type=pl.DeviceIdType.MESH,
            )

        def own(unit):
            if middle:
                begin(along(unit, z, inner, 0, 0))
                if unit < first_ug:
                    begin(along(unit, z, outer, 1, 0))
            else:
                begin(along(unit, z, near, 0, 0))

        def own_rest(unit):
            if whole[unit]:
                begin(along(unit, z, near, 0, 1))

        def from_outer(unit):
            along(unit, outer, z, 0, 0).wait_recv()
            begin(along(unit, outer, inner, 0, 0))
            if not whole[unit]:
                begin(over(unit, outer, r))

        def from_inner(unit, source):
            along(unit, source, z, 0, 0).wait_recv()
            begin(over(unit, source, r))
            if middle and unit < first_ug:
                begin(along(unit, source, outer, 1, 0))

        def need(unit):
            if middle:
                if whole[unit]:
                    along(unit, outer, z, 0, 1).wait_recv()
                else:
                    over(unit, outer, other).wait_recv()
                over(unit, inner, other).wait_recv()
                over(unit, far, other).wait_recv()
            else:
                for source in (near, beyond, far):
                    over(unit, source, other).wait_recv()

        def lower_mix():
            for part in range(3):
                mix_g[z, :, part * channels : (part + 1) * channels] = mix_f[part].astype(jnp.bfloat16)

        def lower_block(block):
            columns = slice(block * LANES, (block + 1) * LANES)
            ug_g[z, block, :, :LANES] = up_f[:, columns].astype(jnp.bfloat16)
            ug_g[z, block, :, LANES:] = gate_f[:, columns].astype(jnp.bfloat16)

        def sums_start(number, summed):
            lane = lax.broadcasted_iota(jnp.int32, (rows, LANES), 1)
            one = jnp.sum(summed, axis=1, keepdims=True)
            two = jnp.sum(summed * summed, axis=1, keepdims=True)
            stats[number, t] = jnp.transpose(jnp.where(lane == 0, one, two))[:8]
            for kind, peer in enumerate((across, diagonal, sibling)):
                begin(summing(number, peer, t, kind))

        def sums_end(number):
            for kind, peer in enumerate((across, diagonal, sibling)):
                summing(number, peer, peer, kind).wait_recv()
            summed = stats[number, 0]
            for slot in range(1, tp):
                summed = summed + stats[number, slot]
            back = jnp.transpose(jnp.concatenate([summed] * (LANES // 8), axis=0))
            average = back[:, 0:1] / full_width
            return average, back[:, 1:2] / full_width - average * average

        def mixer():
            for unit in (0, 1):
                need(unit)
            exchange_end(0)
            gathered = dot32(token_all[0], mix_g[0])
            for slot in range(1, tp):
                gathered = gathered + dot32(token_all[slot], mix_g[slot])
            scaled = [
                (gathered[:, part * channels : (part + 1) * channels] * mixer_scales[part : part + 1])
                .astype(jnp.bfloat16)
                .astype(jnp.float32)
                for part in range(3)
            ]
            mixed = scaled[0] * shifted_mix(
                scaled[1] * scaled[2], mixer_taps[0:1], mixer_taps[1:2], mixer_taps[2:3]
            )
            conv_all[t] = mixed.astype(jnp.bfloat16)
            exchange_start(1)

        def mixer_output():
            need(2)
            exchange_end(1)
            summed = dot32(conv_all[0], out_g[0])
            for slot in range(1, tp):
                summed = summed + dot32(conv_all[slot], out_g[slot])
            summed = summed * out_scale[...] + residual_weight * token_all[t].astype(jnp.float32)
            first_sum[...] = summed
            sums_start(0, summed)

        def first_norm():
            average, spread = sums_end(0)
            norm_all[t] = scaled_norm(
                first_sum[...], average, spread, first_gain[:, own_lanes], first_shift[:, own_lanes]
            ).astype(jnp.bfloat16)

        def guest_copy(part):
            lines = pl.ds(part * guest_rows, guest_rows)
            return pltpu.make_async_remote_copy(
                src_ref=norm_all.at[t, lines],
                dst_ref=guest_all.at[t, lines],
                send_sem=send_g.at[part],
                recv_sem=recv_g.at[part],
                device_id={"fs": outer if middle else near},
                device_id_type=pl.DeviceIdType.MESH,
            )

        def hidden_copy(block):
            return pltpu.make_async_remote_copy(
                src_ref=hidden_out.at[block],
                dst_ref=hidden_all.at[t, block],
                send_sem=send_h.at[block],
                recv_sem=recv_h.at[block],
                device_id={"fs": outer if middle else near},
                device_id_type=pl.DeviceIdType.MESH,
            )

        def units_of(block, left):
            both = dot32(left[0], ug_g[0, block])
            for slot in range(1, tp):
                both = both + dot32(left[slot], ug_g[slot, block])
            columns = slice(block * LANES, (block + 1) * LANES)
            mixed = []
            for side in range(2):
                mixed.append(
                    shifted_mix(
                        both[:, side * LANES : (side + 1) * LANES] * up_scales[side : side + 1, columns],
                        ffn_taps[0, side : side + 1, columns],
                        ffn_taps[1, side : side + 1, columns],
                        ffn_taps[2, side : side + 1, columns],
                    )
                    + ffn_shift[side : side + 1, columns]
                )
            return (mixed[0] * mixed[1] / (1.0 + jnp.exp(-mixed[1]))).astype(jnp.bfloat16)

        def hidden(block):
            hidden_all[t, block] = units_of(block, norm_all)
            exchange_start(first_hidden + block)

        def guest_hidden(block):
            hidden_out[block] = units_of(block, guest_all)
            begin(hidden_copy(block))

        def guest_start(part):
            guest_copy(part).wait_recv()
            exchange_start(first_guest + part)

        def returned(block):
            hidden_copy(block).wait_recv()
            exchange_start(first_hidden + block)

        def down(part):
            need(first_down + part)
            for block in (2 * part, 2 * part + 1):
                exchange_end(first_hidden + block)
            summed = None
            for slot in range(tp):
                left = jnp.concatenate([hidden_all[slot, 2 * part], hidden_all[slot, 2 * part + 1]], axis=1)
                term = dot32(left, down_g[slot, part * 2 * LANES : (part + 1) * 2 * LANES])
                summed = term if summed is None else summed + term
            total[...] = summed if part == 0 else total[...] + summed

        def finish():
            second = total[...] * down_scale[...] + residual_weight * norm_all[t].astype(jnp.float32)
            total[...] = second
            sums_start(1, second)
            for copy in sent[:-3]:
                copy.wait_send()
            average, spread = sums_end(1)
            result[...] = scaled_norm(
                total[...], average, spread, second_gain[:, own_lanes], second_shift[:, own_lanes]
            ).astype(result.dtype)
            for copy in sent[-3:]:
                copy.wait_send()

        def sources_of(unit):
            from_outer(unit)
            from_inner(unit, inner)

        loads[0].wait()
        exchange_start(0)
        for load in loads[1:4]:
            load.wait()
        lower_mix()
        d, u, h, g = first_down, first_ug, first_hidden, first_guest
        if middle:
            own(0)
            own(1)
            loads[4].wait()
            out_g[z] = out_f[...].astype(jnp.bfloat16)
            own(2)
            loads[7].wait()
            down_g[z] = down_f[...].astype(jnp.bfloat16)
            own(d)
            sources_of(0)
            loads[5].wait()
            loads[6].wait()
            lower_block(0)
            lower_block(1)
            own(d + 1)
            sources_of(1)
            from_inner(0, far)
            lower_block(2)
            lower_block(3)
            sources_of(2)
            from_inner(1, far)
            own(d + 2)
            exchange_pass(0)
            lower_block(4)
            lower_block(5)
            from_inner(2, far)
            sources_of(d)
            mixer()
            own(u)
            from_inner(d, far)
            sources_of(d + 1)
            exchange_pass(1)
            mixer_output()
            own(u + 1)
            from_inner(d + 1, far)
            sources_of(d + 2)
            first_norm()
            exchange_start(2)
            own(u + 2)
            from_inner(d + 2, far)
            sources_of(u)
            from_inner(u, far)
            own(u + 3)
            guest_start(0)
            sources_of(u + 1)
            exchange_pass(2)
            exchange_end(2)
            guest_start(1)
            from_inner(u + 1, far)
            own(u + 4)
            need(u)
            hidden(0)
            sources_of(u + 2)
            exchange_pass(g)
            from_inner(u + 2, far)
            own(u + 5)
            need(u + 1)
            hidden(1)
            exchange_pass(g + 1)
            sources_of(u + 3)
            exchange_end(g)
            exchange_end(g + 1)
            guest_hidden(0)
            guest_hidden(1)
            from_inner(u + 3, far)
            exchange_pass(h)
            need(u + 2)
            guest_hidden(2)
            hidden(2)
            exchange_pass(h + 1)
            sources_of(u + 4)
            from_inner(u + 4, far)
            need(u + 3)
            guest_hidden(3)
            hidden(3)
            sources_of(u + 5)
            exchange_pass(h + 2)
            from_inner(u + 5, far)
            need(u + 4)
            guest_hidden(4)
            hidden(4)
            exchange_pass(h + 3)
            down(0)
            need(u + 5)
            guest_hidden(5)
            hidden(5)
            down(1)
            exchange_pass(h + 4)
            exchange_pass(h + 5)
            down(2)
            finish()
        else:
            own(0)
            own_rest(0)
            own(1)
            own_rest(1)
            loads[4].wait()
            out_g[z] = out_f[...].astype(jnp.bfloat16)
            own(2)
            own_rest(2)
            loads[7].wait()
            down_g[z] = down_f[...].astype(jnp.bfloat16)
            for part in range(parts):
                own(d + part)
                own_rest(d + part)
            loads[5].wait()
            loads[6].wait()
            for block in range(blocks):
                lower_block(block)
            own(u)
            own_rest(u)
            from_inner(0, near)
            from_inner(1, near)
            from_inner(0, beyond)
            from_inner(0, far)
            from_inner(1, beyond)
            exchange_pass(0)
            from_inner(1, far)
            from_inner(2, near)
            from_inner(2, beyond)
            from_inner(2, far)
            mixer()
            from_inner(d, near)
            from_inner(d, beyond)
            exchange_pass(1)
            mixer_output()
            first_norm()
            for part in range(GUEST_PARTS):
                begin(guest_copy(part))
            own(u + 1)
            for block in range(1, blocks):
                if block + 1 < blocks:
                    own(u + block + 1)
                own_rest(u + block)
            from_inner(d, far)
            for part in range(1, parts):
                for source in (near, beyond, far):
                    from_inner(d + part, source)
            for block in range(blocks):
                returned(block)
                if block > 0:
                    exchange_pass(h + block - 1)
                if block > 2 and block % 2 == 0:
                    down(block // 2 - 2)
            exchange_pass(h + blocks - 1)
            for part in range(max(parts - 2, 0), parts):
                down(part)
            finish()

    @pl.when(inside)
    def _():
        program(True)

    @pl.when(jnp.logical_not(inside))
    def _():
        program(False)


def fused(
    fs,
    tp,
    tokens,
    outer_gate,
    inner_gate,
    mixer_value,
    mixer_scales,
    mixer_taps,
    mixer_out,
    out_scale,
    first_gain,
    first_shift,
    up_proj,
    gate_proj,
    up_scales,
    ffn_taps,
    ffn_shift,
    down_proj,
    down_scale,
    second_gain,
    second_shift,
):
    rows, own_width = tokens.shape
    depth, channels = outer_gate.shape
    hidden = up_proj.shape[1]
    blocks = hidden // LANES
    count = 3 + blocks + blocks // 2
    moves = 3 + blocks + GUEST_PARTS
    any_space = pl.BlockSpec(memory_space=pl.ANY)
    in_vmem = pl.BlockSpec(memory_space=pltpu.VMEM)

    def row(vector):
        return vector.reshape(1, -1)

    return pl.pallas_call(
        functools.partial(kernel, fs, tp),
        out_shape=jax.ShapeDtypeStruct((rows, own_width), jnp.bfloat16),
        in_specs=[any_space] * 8 + [in_vmem] * 11,
        out_specs=in_vmem,
        scratch_shapes=[
            pltpu.VMEM((3, depth, channels), jnp.float32),
            pltpu.VMEM(mixer_out.shape, jnp.float32),
            pltpu.VMEM(up_proj.shape, jnp.float32),
            pltpu.VMEM(gate_proj.shape, jnp.float32),
            pltpu.VMEM(down_proj.shape, jnp.float32),
            pltpu.VMEM((fs, depth, 3 * channels), jnp.bfloat16),
            pltpu.VMEM((fs,) + mixer_out.shape, jnp.bfloat16),
            pltpu.VMEM((fs, blocks, depth, 2 * LANES), jnp.bfloat16),
            pltpu.VMEM((fs,) + down_proj.shape, jnp.bfloat16),
            pltpu.VMEM((tp, rows, own_width), jnp.bfloat16),
            pltpu.VMEM((tp, rows, channels), jnp.bfloat16),
            pltpu.VMEM((tp, rows, own_width), jnp.bfloat16),
            pltpu.VMEM((tp, rows, own_width), jnp.bfloat16),
            pltpu.VMEM((tp, blocks, rows, LANES), jnp.bfloat16),
            pltpu.VMEM((blocks, rows, LANES), jnp.bfloat16),
            pltpu.VMEM((rows, own_width), jnp.float32),
            pltpu.VMEM((rows, own_width), jnp.float32),
            pltpu.VMEM((2, tp, 8, rows), jnp.float32),
            pltpu.SemaphoreType.DMA((8,)),
            pltpu.SemaphoreType.DMA((count, fs, 2, 2)),
            pltpu.SemaphoreType.DMA((count, fs)),
            pltpu.SemaphoreType.DMA((count, fs, 2)),
            pltpu.SemaphoreType.DMA((count, fs)),
            pltpu.SemaphoreType.DMA((moves, 3)),
            pltpu.SemaphoreType.DMA((moves, tp)),
            pltpu.SemaphoreType.DMA((2, 3)),
            pltpu.SemaphoreType.DMA((2, tp)),
            pltpu.SemaphoreType.DMA((GUEST_PARTS,)),
            pltpu.SemaphoreType.DMA((GUEST_PARTS,)),
            pltpu.SemaphoreType.DMA((blocks,)),
            pltpu.SemaphoreType.DMA((blocks,)),
        ],
        compiler_params=pltpu.CompilerParams(
            collective_id=0, has_side_effects=True, vmem_limit_bytes=60 * 1024 * 1024
        ),
    )(
        tokens,
        outer_gate,
        inner_gate,
        mixer_value,
        mixer_out,
        up_proj,
        gate_proj,
        down_proj,
        mixer_scales,
        mixer_taps,
        row(out_scale),
        row(first_gain),
        row(first_shift),
        up_scales,
        ffn_taps,
        ffn_shift,
        row(down_scale),
        row(second_gain),
        row(second_shift),
    )


def fits(mesh):
    return mesh.shape["rep"] == 2 and mesh.shape["fs"] == 4 and mesh.shape["tp"] == 4


def solution(mesh):
    body = functools.partial(fused, mesh.shape["fs"], mesh.shape["tp"]) if fits(mesh) else local
    return jax.shard_map(
        body,
        mesh=mesh,
        in_specs=(
            P(("rep", "fs"), "tp"),
            P("fs", "tp"),
            P("fs", "tp"),
            P("fs", "tp"),
            P(None, "tp"),
            P(None, "tp"),
            P("fs", "tp"),
            P("tp"),
            P(),
            P(),
            P("fs", "tp"),
            P("fs", "tp"),
            P(None, "tp"),
            P(None, None, "tp"),
            P(None, "tp"),
            P("fs", "tp"),
            P("tp"),
            P(),
            P(),
        ),
        out_specs=P(("rep", "fs"), "tp"),
        check_vma=False,
    )
```

time: 135 us -> 117 us (0.87)
  Pallas kernels: 125 us -> 115 us
  local copies, waits for them, and re-layouts: 7.05 us -> 1.87 us
  other arithmetic: 2.64 us -> 0 us
    pallas_call x1, Pallas kernels: 125 us -> 115 us  [fused(): pl.pallas_call(functools.partial(kernel, fs, tp), out_shape=jax.ShapeDtyp...]
    dynamic_slice x4 -> x0, local copies, waits for them, and re-layouts: 3.04 us -> none  [own_columns(): lax.dynamic_slice_in_dim(vector, lax.axis_index('tp') * own_width, own_wi...]
    concatenate x2 -> x0, other arithmetic: 2.64 us -> none  [the longest x1 1.35 us: fused(): jnp.concatenate([up_scales, ffn_taps[:, 0], ffn_taps[:, 1], ffn_shift], a...]
where the time goes in v1:
time: 117 us
  Pallas kernels  115 us (98%)
  local copies, waits for them, and re-layouts  1.87 us (2%)
    pallas_call x1, Pallas kernels, fused(): pl.pallas_call(functools.partial(kernel, fs, tp), out_shape=jax.ShapeDtyp...  115 us

profile of v1, /device:TPU:0, one launch (start us, length us, event | category | flops | bytes accessed | tf_op | source)
XLA Modules:
  0.0 117.2 jit_solution(4713389914317406843)
XLA Ops:
  0.0 115.3 %shard_map.181 = bf16[512,512]{1,0:T(8,128)(2,1)} custom-call(bf16[512,512]{1,0:T(8,128)(2,1)} %tokens_hbm.1, f32[512,128]{1,0:T(8,128)} %outer_hbm.1, f32[512,128]{1,0:T(8,128)} %inner_hbm.1, f32[512,128]{1,0:T(8,128)} %value_hbm.1, f32[128,512]{1,0:T(8,128)} %out_hbm.1, f32[512,768]{1,0:T(8,128)} %up_hbm.1, f32[512,768]{1,0:T(8,128)} %gate_hbm.1, ...), custom_call_target="tpu_custom_call" | custom-call | tf_op jit(solution)/shard_map/pallas_call | solution.py:748
  115.3 1.9 %copy.21 = bf16[512,512]{1,0:T(8,128)(2,1)} copy(bf16[512,512]{1,0:T(8,128)(2,1)} %shard_map.181) | data formatting | bytes 1048576

commit v2 on v1

v2 whole, which is shorter than its diff:
```python
import functools

import jax
import jax.numpy as jnp
from jax import lax
from jax.experimental import pallas as pl
from jax.experimental.pallas import tpu as pltpu
from jax.sharding import PartitionSpec as P

LEN = 128


norm_eps = 1e-05
residual_weight = 8.0**0.25


def causal_mix(signal, kernel_taps):
    sequences = signal.reshape(-1, LEN, signal.shape[-1])
    padded = jnp.pad(sequences, ((0, 0), (2, 0), (0, 0)))
    mixed = (
        kernel_taps[0] * padded[:, :-2]
        + kernel_taps[1] * padded[:, 1:-1]
        + kernel_taps[2] * padded[:, 2:]
    )
    return mixed.reshape(signal.shape)


def lowered(matrix):
    return matrix.astype(jnp.bfloat16)


def single_fold(operand, portion):
    return jnp.dot(operand, portion, preferred_element_type=jnp.float32)


def fold_step(operand, pieces):
    result = []
    for number in range(len(pieces)):
        result.append(jnp.dot(operand, pieces[number], preferred_element_type=jnp.float32))
    return tuple(result)


def own_columns(vector, own_width):
    return lax.dynamic_slice_in_dim(vector, lax.axis_index("tp") * own_width, own_width, 0)


def scaled_norm(summed, average, spread, gain_vector, shift_vector):
    return (summed - average) * lax.rsqrt(spread + norm_eps) * gain_vector + shift_vector


def local(
    tokens,
    outer_gate,
    inner_gate,
    mixer_value,
    mixer_scales,
    mixer_taps,
    mixer_out,
    out_scale,
    first_gain,
    first_shift,
    up_proj,
    gate_proj,
    up_scales,
    ffn_taps,
    ffn_shift,
    down_proj,
    down_scale,
    second_gain,
    second_shift,
):
    own_width = tokens.shape[1]
    full_width = own_width * lax.axis_size("tp")
    token_whole = lax.all_gather(tokens, "tp", axis=1, tiled=True)
    outer_part, inner_part, value_part = fold_step(
        token_whole,
        (
            lax.all_gather(lowered(outer_gate), "fs", axis=0, tiled=True),
            lax.all_gather(lowered(inner_gate), "fs", axis=0, tiled=True),
            lax.all_gather(lowered(mixer_value), "fs", axis=0, tiled=True),
        ),
    )
    outer_part = (outer_part * mixer_scales[0]).astype(jnp.bfloat16)
    inner_part = (inner_part * mixer_scales[1]).astype(jnp.bfloat16)
    value_part = (value_part * mixer_scales[2]).astype(jnp.bfloat16)
    product = inner_part.astype(jnp.float32) * value_part.astype(jnp.float32)
    mixed_conv = (outer_part.astype(jnp.float32) * causal_mix(product, mixer_taps)).astype(
        jnp.bfloat16
    )
    conv_whole = lax.all_gather(mixed_conv, "tp", axis=1, tiled=True)
    mixer_sum = (
        single_fold(conv_whole, lax.all_gather(lowered(mixer_out), "fs", axis=0, tiled=True))
        * out_scale
    )
    first_sum = residual_weight * tokens.astype(jnp.float32) + mixer_sum
    row_total, row_square = lax.psum(
        (jnp.sum(first_sum, 1, keepdims=True), jnp.sum(first_sum * first_sum, 1, keepdims=True)),
        "tp",
    )
    average = row_total / full_width
    spread = row_square / full_width - average * average
    normed = scaled_norm(
        first_sum,
        average,
        spread,
        own_columns(first_gain, own_width),
        own_columns(first_shift, own_width),
    ).astype(jnp.bfloat16)
    normed_whole = lax.all_gather(normed, "tp", axis=1, tiled=True)
    up_matrix, gate_matrix = (
        lax.all_gather(lowered(up_proj), "fs", axis=0, tiled=True),
        lax.all_gather(lowered(gate_proj), "fs", axis=0, tiled=True),
    )
    up_linear = jnp.dot(normed_whole, up_matrix, preferred_element_type=jnp.float32)
    gate_linear = jnp.dot(normed_whole, gate_matrix, preferred_element_type=jnp.float32)
    up_linear = up_linear * up_scales[0]
    gate_linear = gate_linear * up_scales[1]
    up_mixed = causal_mix(up_linear, ffn_taps[:, 0]) + ffn_shift[0]
    gate_mixed = causal_mix(gate_linear, ffn_taps[:, 1]) + ffn_shift[1]
    hidden = (up_mixed * jax.nn.silu(gate_mixed)).astype(jnp.bfloat16)
    hidden_whole = lax.all_gather(hidden, "tp", axis=1, tiled=True)
    ffn_sum = (
        single_fold(hidden_whole, lax.all_gather(lowered(down_proj), "fs", axis=0, tiled=True))
        * down_scale
    )
    second_sum = residual_weight * normed.astype(jnp.float32) + ffn_sum
    second_total, second_square = lax.psum(
        (jnp.sum(second_sum, 1, keepdims=True), jnp.sum(second_sum * second_sum, 1, keepdims=True)),
        "tp",
    )
    second_average = second_total / full_width
    second_spread = second_square / full_width - second_average * second_average
    return scaled_norm(
        second_sum,
        second_average,
        second_spread,
        own_columns(second_gain, own_width),
        own_columns(second_shift, own_width),
    ).astype(jnp.bfloat16)


LANES = 128
STAT_ROWS = 8
GUEST_PARTS = 2
RETURN_PARTS = 2
MIX_PARTS = 4
BLOCK_PARTS = (1, 1, 1, 1, 1, 2)
LANE_DEPTH = {"zi": 14, "zo": 8, "y": 8, "x": 8, "d": 8}


def shifted_mix(signal, first, second, third):
    rows = lax.broadcasted_iota(jnp.int32, signal.shape, 0) % LEN
    one = jnp.where(rows >= 1, pltpu.roll(signal, 1, 0), 0.0)
    two = jnp.where(rows >= 2, pltpu.roll(signal, 2, 0), 0.0)
    return first * two + second * one + third * signal


def dot32(left, right):
    return jnp.dot(left, right, preferred_element_type=jnp.float32)


def kernel(
    fs,
    tp,
    tokens_hbm,
    outer_hbm,
    inner_hbm,
    value_hbm,
    out_hbm,
    up_hbm,
    gate_hbm,
    down_hbm,
    mixer_scales_hbm,
    mixer_taps_hbm,
    out_scale_hbm,
    first_gain_hbm,
    first_shift_hbm,
    up_scales_hbm,
    ffn_taps_hbm,
    ffn_shift_hbm,
    down_scale_hbm,
    second_gain_hbm,
    second_shift_hbm,
    result,
    mix_f,
    out_f,
    up_f,
    gate_f,
    down_f,
    mixer_scales,
    mixer_taps,
    out_scale,
    first_gain,
    first_shift,
    up_scales,
    ffn_taps,
    ffn_shift,
    down_scale,
    second_gain,
    second_shift,
    mix_g,
    out_g,
    ug_g,
    down_g,
    token_all,
    conv_all,
    norm_all,
    guest_all,
    hidden_all,
    hidden_out,
    first_sum,
    total,
    stats,
    load_sem,
    send_sem,
    arrive_sem,
    gather_sem,
    recv_x,
    recv_s,
    recv_g,
    recv_h,
):
    r, z, t = lax.axis_index("rep"), lax.axis_index("fs"), lax.axis_index("tp")
    sibling = t + 1 - 2 * (t % 2)
    across = (t + 2) % tp
    diagonal = (sibling + 2) % tp
    other = 1 - r
    rows, own_width = result.shape
    full_width = own_width * tp
    channels = conv_all.shape[2]
    blocks = ug_g.shape[1]
    last = fs - 1
    own_lanes = pl.ds(pl.multiple_of(t * own_width, own_width), own_width)

    sources = (tokens_hbm, outer_hbm, inner_hbm, value_hbm, out_hbm, up_hbm, gate_hbm, down_hbm)
    sources += (mixer_scales_hbm, mixer_taps_hbm, out_scale_hbm, first_gain_hbm.at[:, own_lanes])
    sources += (first_shift_hbm.at[:, own_lanes], up_scales_hbm, ffn_taps_hbm, ffn_shift_hbm, down_scale_hbm)
    sources += (second_gain_hbm.at[:, own_lanes], second_shift_hbm.at[:, own_lanes])
    places = (token_all.at[t], mix_f.at[0], mix_f.at[1], mix_f.at[2], out_f, up_f, gate_f, down_f)
    places += (mixer_scales, mixer_taps, out_scale, first_gain, first_shift, up_scales, ffn_taps, ffn_shift)
    places += (down_scale, second_gain, second_shift)
    loads = [
        pltpu.make_async_copy(source, place, load_sem.at[number])
        for number, (source, place) in enumerate(zip(sources, places))
    ]
    for load in loads:
        load.start()

    barrier = pltpu.get_barrier_semaphore()
    for peer in (sibling, across, diagonal):
        pl.semaphore_signal(barrier, inc=1, device_id={"tp": peer}, device_id_type=pl.DeviceIdType.MESH)
    pl.semaphore_signal(barrier, inc=1, device_id={"rep": other}, device_id_type=pl.DeviceIdType.MESH)

    @pl.when(z > 0)
    def _():
        pl.semaphore_signal(barrier, inc=1, device_id={"fs": z - 1}, device_id_type=pl.DeviceIdType.MESH)

    @pl.when(z < last)
    def _():
        pl.semaphore_signal(barrier, inc=1, device_id={"fs": z + 1}, device_id_type=pl.DeviceIdType.MESH)

    inside = (z > 0) & (z < last)

    @pl.when(inside)
    def _():
        pl.semaphore_wait(barrier, 6)

    @pl.when(jnp.logical_not(inside))
    def _():
        pl.semaphore_wait(barrier, 5)

    guest_rows = rows // GUEST_PARTS
    return_rows = rows // RETURN_PARTS
    first_hidden, first_guest = 3, 3 + blocks * RETURN_PARTS

    def offset(value, size):
        return value if isinstance(value, int) else pl.multiple_of(value, size)

    def mix_unit(part):
        size = mix_g.shape[1] // (2 * MIX_PARTS)
        return lambda source, half: mix_g.at[source, pl.ds(offset((part * 2 + half) * size, size), size)]

    def out_unit(source, half):
        size = out_g.shape[1] // 2
        return out_g.at[source, pl.ds(offset(half * size, size), size)]

    def ug_unit(block, part):
        size = ug_g.shape[2] // (2 * BLOCK_PARTS[block])
        return lambda source, half: ug_g.at[
            source, block, pl.ds(offset((part * 2 + half) * size, size), size)
        ]

    def down_unit(part):
        size = LANES
        return lambda source, half: down_g.at[source, pl.ds(offset((part * 2 + half) * size, size), size)]

    parts = blocks // 2
    units = [mix_unit(part) for part in range(MIX_PARTS)] + [out_unit]
    out_index, first_down = MIX_PARTS, MIX_PARTS + 1
    units += [down_unit(part) for part in range(parts)]
    first_ug = len(units)
    block_units = []
    for block in range(blocks):
        block_units.append(range(len(units), len(units) + BLOCK_PARTS[block]))
        units += [ug_unit(block, part) for part in range(BLOCK_PARTS[block])]
    count = len(units)

    def program(middle):
        if middle:
            outer, inner, far = (z - 1) * last, last - z, (2 - z) * last
        else:
            near = 1 + z // last
            beyond, far = last - near, last - z
        queues, lowered_blocks = {name: [] for name in LANE_DEPTH}, []
        bases = {}
        for name, depth in LANE_DEPTH.items():
            bases[name] = sum(LANE_DEPTH[other_name] for other_name in bases)

        def send(lane, source, target, recv_sem, device):
            queue, depth = queues[lane], LANE_DEPTH[lane]
            if len(queue) >= depth:
                queue[-depth].wait_send()
            copy = pltpu.make_async_remote_copy(
                src_ref=source,
                dst_ref=target,
                send_sem=send_sem.at[bases[lane] + len(queue) % depth],
                recv_sem=recv_sem,
                device_id=device,
                device_id_type=pl.DeviceIdType.MESH,
            )
            copy.start()
            queue.append(copy)

        def arrived(ref, recv_sem):
            pltpu.make_async_remote_copy(
                src_ref=ref,
                dst_ref=ref,
                send_sem=send_sem.at[0],
                recv_sem=recv_sem,
                device_id={"tp": sibling},
                device_id_type=pl.DeviceIdType.MESH,
            ).wait_recv()

        def moved(number, slot):
            if number < 3:
                return (token_all, conv_all, norm_all)[number].at[slot]
            if number >= first_guest:
                return guest_all.at[slot, pl.ds((number - first_guest) * guest_rows, guest_rows)]
            block, part = (number - first_hidden) // RETURN_PARTS, (number - first_hidden) % RETURN_PARTS
            if middle:
                return hidden_all.at[slot, block]
            return hidden_all.at[slot, block, pl.ds(part * return_rows, return_rows)]

        def exchange_start(number):
            if number == 0:
                loads[0].wait()
            send("x", moved(number, t), moved(number, t), recv_x.at[number, 0], {"tp": across})
            send("d", moved(number, t), moved(number, t), recv_x.at[number, 1], {"tp": sibling})

        def exchange_pass(number):
            arrived(moved(number, across), recv_x.at[number, 0])
            send("d", moved(number, across), moved(number, across), recv_x.at[number, 1], {"tp": sibling})

        def exchange_end(number):
            arrived(moved(number, pl.ds(0, 2)), recv_x.at[number, 1])

        def own(unit):
            ref = units[unit](z, r)
            if middle:
                send("zi", ref, ref, arrive_sem.at[unit, 1], {"fs": inner})
                if unit < first_ug:
                    send("zo", ref, ref, arrive_sem.at[unit, 0], {"fs": outer})
            else:
                send("zi", ref, ref, arrive_sem.at[unit, 0], {"fs": near})

        def own_rest(unit):
            ref = units[unit](z, other)
            send("zi", ref, ref, gather_sem.at[unit], {"fs": near})

        def from_outer(unit):
            ref = units[unit](outer, r)
            arrived(ref, arrive_sem.at[unit, 0])
            send("zi", ref, ref, arrive_sem.at[unit, 2], {"fs": inner})

        def from_inner(unit, source, place):
            ref = units[unit](source, r)
            arrived(ref, arrive_sem.at[unit, place])
            send("y", ref, ref, gather_sem.at[unit], {"rep": other})
            if middle and unit < first_ug:
                send("zo", ref, ref, arrive_sem.at[unit, place], {"fs": outer})

        def need(unit):
            arrived(units[unit](pl.ds(0, 3), 0), gather_sem.at[unit])

        def lower_mix():
            for load in loads[1:4]:
                load.wait()
            for part in range(3):
                mix_g[z, :, part * channels : (part + 1) * channels] = mix_f[part].astype(jnp.bfloat16)

        def lower_out():
            loads[4].wait()
            out_g[z] = out_f[...].astype(jnp.bfloat16)

        def lower_down():
            loads[7].wait()
            down_g[z] = down_f[...].astype(jnp.bfloat16)

        def small_loads():
            for load in loads[8:]:
                load.wait()

        def lower_block(block):
            if not lowered_blocks:
                loads[5].wait()
                loads[6].wait()
            lowered_blocks.append(block)
            columns = slice(block * LANES, (block + 1) * LANES)
            ug_g[z, block, :, :LANES] = up_f[:, columns].astype(jnp.bfloat16)
            ug_g[z, block, :, LANES:] = gate_f[:, columns].astype(jnp.bfloat16)

        def sums_start(number, summed):
            lane = lax.broadcasted_iota(jnp.int32, (rows, LANES), 1)
            one = jnp.sum(summed, axis=1, keepdims=True)
            two = jnp.sum(summed * summed, axis=1, keepdims=True)
            stats[number, t] = jnp.transpose(jnp.where(lane == 0, one, two))[:STAT_ROWS]
            ref = stats.at[number, t]
            for lane_name, peer in (("x", across), ("x", diagonal), ("d", sibling)):
                send(lane_name, ref, ref, recv_s.at[number], {"tp": peer})

        def sums_end(number):
            arrived(stats.at[number, pl.ds(0, 3)], recv_s.at[number])
            summed = stats[number, 0]
            for slot in range(1, tp):
                summed = summed + stats[number, slot]
            back = jnp.transpose(jnp.concatenate([summed] * (LANES // STAT_ROWS), axis=0))
            average = back[:, 0:1] / full_width
            return average, back[:, 1:2] / full_width - average * average

        def mixer():
            for unit in range(MIX_PARTS):
                need(unit)
            exchange_end(0)
            gathered = dot32(token_all[0], mix_g[0])
            for slot in range(1, tp):
                gathered = gathered + dot32(token_all[slot], mix_g[slot])
            scaled = [
                (gathered[:, part * channels : (part + 1) * channels] * mixer_scales[part : part + 1])
                .astype(jnp.bfloat16)
                .astype(jnp.float32)
                for part in range(3)
            ]
            mixed = scaled[0] * shifted_mix(
                scaled[1] * scaled[2], mixer_taps[0:1], mixer_taps[1:2], mixer_taps[2:3]
            )
            conv_all[t] = mixed.astype(jnp.bfloat16)
            exchange_start(1)

        def mixer_output():
            need(out_index)
            exchange_end(1)
            summed = dot32(conv_all[0], out_g[0])
            for slot in range(1, tp):
                summed = summed + dot32(conv_all[slot], out_g[slot])
            summed = summed * out_scale[...] + residual_weight * token_all[t].astype(jnp.float32)
            first_sum[...] = summed
            sums_start(0, summed)

        def first_norm():
            average, spread = sums_end(0)
            norm_all[t] = scaled_norm(
                first_sum[...], average, spread, first_gain[...], first_shift[...]
            ).astype(jnp.bfloat16)

        def guest_send(part):
            lines = pl.ds(part * guest_rows, guest_rows)
            send("zi", norm_all.at[t, lines], guest_all.at[t, lines], recv_g.at[part], {"fs": near})

        def units_of(block, left):
            both = dot32(left(0), ug_g[0, block])
            for slot in range(1, tp):
                both = both + dot32(left(slot), ug_g[slot, block])
            columns = slice(block * LANES, (block + 1) * LANES)
            mixed = []
            for side in range(2):
                mixed.append(
                    shifted_mix(
                        both[:, side * LANES : (side + 1) * LANES] * up_scales[side : side + 1, columns],
                        ffn_taps[0, side : side + 1, columns],
                        ffn_taps[1, side : side + 1, columns],
                        ffn_taps[2, side : side + 1, columns],
                    )
                    + ffn_shift[side : side + 1, columns]
                )
            return (mixed[0] * mixed[1] / (1.0 + jnp.exp(-mixed[1]))).astype(jnp.bfloat16)

        def need_block(block):
            for unit in block_units[block]:
                need(unit)

        def hidden(block):
            hidden_all[t, block] = units_of(block, lambda slot: norm_all[slot])
            exchange_start(first_hidden + block * RETURN_PARTS)

        def give_back(block):
            for part in range(RETURN_PARTS):
                lines = pl.ds(part * return_rows, return_rows)
                number = block * RETURN_PARTS + part
                send(
                    "zo", hidden_out.at[block, lines], hidden_all.at[t, block, lines], recv_h.at[number], {"fs": outer}
                )

        def guest_hidden(block):
            hidden_out[block] = units_of(block, lambda slot: guest_all[slot])
            give_back(block)

        def both_hidden(block):
            units_both = units_of(block, lambda slot: jnp.concatenate([guest_all[slot], norm_all[slot]], axis=0))
            hidden_out[block] = units_both[:rows]
            hidden_all[t, block] = units_both[rows:]
            give_back(block)
            exchange_start(first_hidden + block * RETURN_PARTS)

        def guest_start(part):
            lines = pl.ds(part * guest_rows, guest_rows)
            arrived(guest_all.at[t, lines], recv_g.at[part])
            exchange_start(first_guest + part)

        def returned(number):
            arrived(moved(first_hidden + number, t), recv_h.at[number])
            exchange_start(first_hidden + number)

        def hidden_end(block):
            for part in range(1 if middle else RETURN_PARTS):
                exchange_end(first_hidden + block * RETURN_PARTS + part)

        def down(part):
            need(first_down + part)
            for block in (2 * part, 2 * part + 1):
                hidden_end(block)
            summed = None
            for slot in range(tp):
                left = jnp.concatenate([hidden_all[slot, 2 * part], hidden_all[slot, 2 * part + 1]], axis=1)
                term = dot32(left, down_g[slot, part * 2 * LANES : (part + 1) * 2 * LANES])
                summed = term if summed is None else summed + term
            total[...] = summed if part == 0 else total[...] + summed

        def finish():
            second = total[...] * down_scale[...] + residual_weight * norm_all[t].astype(jnp.float32)
            total[...] = second
            sums_start(1, second)
            average, spread = sums_end(1)
            result[...] = scaled_norm(total[...], average, spread, second_gain[...], second_shift[...]).astype(
                result.dtype
            )
            for name, queue in queues.items():
                for copy in queue[-LANE_DEPTH[name] :]:
                    copy.wait_send()

        if middle:
            lower_mix()
            own(0)
            lower_out()
            own(2)
            own(1)
            exchange_start(0)
            own(3)
            from_outer(0)
            lower_down()
            from_inner(0, inner, 1)
            from_inner(2, inner, 1)
            from_outer(2)
            from_inner(1, inner, 1)
            from_outer(3)
            lower_block(3)
            from_outer(1)
            own(4)
            from_inner(0, far, 2)
            lower_block(5)
            small_loads()
            from_inner(3, inner, 1)
            from_inner(2, far, 2)
            lower_block(1)
            lower_block(0)
            own(9)
            from_inner(3, far, 2)
            from_outer(4)
            lower_block(4)
            from_inner(1, far, 2)
            own(8)
            exchange_pass(0)
            own(5)
            from_inner(4, inner, 1)
            from_inner(9, inner, 1)
            mixer()
            from_inner(4, far, 2)
            from_inner(8, inner, 1)
            own(11)
            own(14)
            from_inner(5, inner, 1)
            own(7)
            exchange_pass(1)
            lower_block(2)
            mixer_output()
            from_inner(11, inner, 1)
            from_outer(9)
            from_inner(14, inner, 1)
            first_norm()
            own(12)
            own(6)
            exchange_start(2)
            from_inner(7, inner, 1)
            from_inner(9, far, 2)
            from_outer(7)
            from_inner(12, inner, 1)
            from_inner(6, inner, 1)
            from_outer(8)
            own(10)
            from_inner(7, far, 2)
            from_outer(10)
            guest_start(0)
            from_outer(6)
            from_outer(5)
            exchange_pass(2)
            from_inner(8, far, 2)
            from_outer(13)
            guest_start(1)
            exchange_end(2)
            from_inner(10, inner, 1)
            from_outer(11)
            exchange_pass(15)
            from_inner(10, far, 2)
            from_inner(6, far, 2)
            exchange_pass(16)
            from_inner(5, far, 2)
            from_outer(12)
            own(13)
            from_inner(13, far, 2)
            need_block(0)
            exchange_end(15)
            exchange_end(16)
            need_block(1)
            both_hidden(1)
            from_inner(11, far, 2)
            from_outer(14)
            both_hidden(0)
            need_block(2)
            from_inner(12, far, 2)
            both_hidden(2)
            from_inner(13, inner, 1)
            need_block(3)
            both_hidden(3)
            from_inner(14, far, 2)
            exchange_pass(5)
            need_block(4)
            both_hidden(4)
            need_block(5)
            both_hidden(5)
            exchange_pass(11)
            exchange_pass(7)
            exchange_pass(3)
            exchange_pass(9)
            exchange_pass(13)
            down(0)
            down(1)
            down(2)
            finish()
        else:
            lower_mix()
            own(0)
            lower_out()
            own(3)
            own(2)
            own(1)
            own(4)
            lower_down()
            lower_block(3)
            own_rest(3)
            exchange_start(0)
            small_loads()
            from_inner(0, near, 0)
            own_rest(1)
            from_inner(2, near, 0)
            from_inner(3, near, 0)
            own_rest(2)
            lower_block(1)
            own_rest(0)
            from_inner(0, beyond, 1)
            lower_block(2)
            own(5)
            from_inner(2, beyond, 1)
            own(10)
            from_inner(1, beyond, 1)
            lower_block(5)
            from_inner(1, near, 0)
            own(9)
            from_inner(0, far, 2)
            from_inner(3, beyond, 1)
            own_rest(4)
            lower_block(0)
            from_inner(2, far, 2)
            own(6)
            from_inner(3, far, 2)
            exchange_pass(0)
            from_inner(1, far, 2)
            own(11)
            mixer()
            from_inner(4, near, 0)
            from_inner(4, beyond, 1)
            from_inner(4, far, 2)
            own(13)
            own(7)
            exchange_pass(1)
            lower_block(4)
            own(8)
            mixer_output()
            first_norm()
            guest_send(0)
            guest_send(1)
            from_inner(5, beyond, 1)
            from_inner(5, near, 0)
            own_rest(9)
            own(14)
            from_inner(6, near, 0)
            own(12)
            from_inner(7, beyond, 1)
            own_rest(8)
            from_inner(7, far, 2)
            own_rest(11)
            own_rest(10)
            from_inner(7, near, 0)
            own_rest(14)
            own_rest(12)
            returned(2)
            from_inner(5, far, 2)
            returned(3)
            own_rest(13)
            returned(0)
            returned(1)
            exchange_pass(6)
            from_inner(6, beyond, 1)
            returned(4)
            own_rest(6)
            returned(5)
            returned(6)
            exchange_pass(5)
            own_rest(5)
            from_inner(6, far, 2)
            exchange_pass(4)
            own_rest(7)
            returned(7)
            returned(8)
            returned(9)
            exchange_pass(3)
            returned(10)
            exchange_pass(10)
            exchange_pass(8)
            exchange_pass(7)
            exchange_pass(11)
            returned(11)
            exchange_pass(9)
            exchange_pass(12)
            exchange_pass(13)
            down(0)
            exchange_pass(14)
            down(1)
            down(2)
            finish()
    @pl.when(inside)
    def _():
        program(True)

    @pl.when(jnp.logical_not(inside))
    def _():
        program(False)


def fused(
    fs,
    tp,
    tokens,
    outer_gate,
    inner_gate,
    mixer_value,
    mixer_scales,
    mixer_taps,
    mixer_out,
    out_scale,
    first_gain,
    first_shift,
    up_proj,
    gate_proj,
    up_scales,
    ffn_taps,
    ffn_shift,
    down_proj,
    down_scale,
    second_gain,
    second_shift,
):
    rows, own_width = tokens.shape
    depth, channels = outer_gate.shape
    hidden = up_proj.shape[1]
    blocks = hidden // LANES
    count = MIX_PARTS + 1 + blocks // 2 + sum(BLOCK_PARTS)
    moves = 3 + blocks * RETURN_PARTS + GUEST_PARTS
    any_space = pl.BlockSpec(memory_space=pl.ANY)
    in_vmem = pl.BlockSpec(memory_space=pltpu.VMEM)

    def row(vector):
        return vector.reshape(1, -1)

    return pl.pallas_call(
        functools.partial(kernel, fs, tp),
        out_shape=jax.ShapeDtypeStruct((rows, own_width), jnp.bfloat16),
        in_specs=[any_space] * 19,
        out_specs=in_vmem,
        scratch_shapes=[
            pltpu.VMEM((3, depth, channels), jnp.float32),
            pltpu.VMEM(mixer_out.shape, jnp.float32),
            pltpu.VMEM(up_proj.shape, jnp.float32),
            pltpu.VMEM(gate_proj.shape, jnp.float32),
            pltpu.VMEM(down_proj.shape, jnp.float32),
            pltpu.VMEM(mixer_scales.shape, jnp.float32),
            pltpu.VMEM(mixer_taps.shape, jnp.float32),
            pltpu.VMEM((1, own_width), jnp.float32),
            pltpu.VMEM((1, own_width), jnp.float32),
            pltpu.VMEM((1, own_width), jnp.float32),
            pltpu.VMEM(up_scales.shape, jnp.float32),
            pltpu.VMEM(ffn_taps.shape, jnp.float32),
            pltpu.VMEM(ffn_shift.shape, jnp.float32),
            pltpu.VMEM((1, own_width), jnp.float32),
            pltpu.VMEM((1, own_width), jnp.float32),
            pltpu.VMEM((1, own_width), jnp.float32),
            pltpu.VMEM((fs, depth, 3 * channels), jnp.bfloat16),
            pltpu.VMEM((fs,) + mixer_out.shape, jnp.bfloat16),
            pltpu.VMEM((fs, blocks, depth, 2 * LANES), jnp.bfloat16),
            pltpu.VMEM((fs,) + down_proj.shape, jnp.bfloat16),
            pltpu.VMEM((tp, rows, own_width), jnp.bfloat16),
            pltpu.VMEM((tp, rows, channels), jnp.bfloat16),
            pltpu.VMEM((tp, rows, own_width), jnp.bfloat16),
            pltpu.VMEM((tp, rows, own_width), jnp.bfloat16),
            pltpu.VMEM((tp, blocks, rows, LANES), jnp.bfloat16),
            pltpu.VMEM((blocks, rows, LANES), jnp.bfloat16),
            pltpu.VMEM((rows, own_width), jnp.float32),
            pltpu.VMEM((rows, own_width), jnp.float32),
            pltpu.VMEM((2, tp, STAT_ROWS, rows), jnp.float32),
            pltpu.SemaphoreType.DMA((19,)),
            pltpu.SemaphoreType.DMA((sum(LANE_DEPTH.values()),)),
            pltpu.SemaphoreType.DMA((count, 3)),
            pltpu.SemaphoreType.DMA((count,)),
            pltpu.SemaphoreType.DMA((moves, 2)),
            pltpu.SemaphoreType.DMA((2,)),
            pltpu.SemaphoreType.DMA((GUEST_PARTS,)),
            pltpu.SemaphoreType.DMA((blocks * RETURN_PARTS,)),
        ],
        compiler_params=pltpu.CompilerParams(
            collective_id=0, has_side_effects=True, vmem_limit_bytes=60 * 1024 * 1024
        ),
    )(
        tokens,
        outer_gate,
        inner_gate,
        mixer_value,
        mixer_out,
        up_proj,
        gate_proj,
        down_proj,
        mixer_scales,
        mixer_taps,
        row(out_scale),
        row(first_gain),
        row(first_shift),
        up_scales,
        ffn_taps,
        ffn_shift,
        row(down_scale),
        row(second_gain),
        row(second_shift),
    )


def fits(mesh):
    return mesh.shape["rep"] == 2 and mesh.shape["fs"] == 4 and mesh.shape["tp"] == 4


def solution(mesh):
    body = functools.partial(fused, mesh.shape["fs"], mesh.shape["tp"]) if fits(mesh) else local
    return jax.shard_map(
        body,
        mesh=mesh,
        in_specs=(
            P(("rep", "fs"), "tp"),
            P("fs", "tp"),
            P("fs", "tp"),
            P("fs", "tp"),
            P(None, "tp"),
            P(None, "tp"),
            P("fs", "tp"),
            P("tp"),
            P(),
            P(),
            P("fs", "tp"),
            P("fs", "tp"),
            P(None, "tp"),
            P(None, None, "tp"),
            P(None, "tp"),
            P("fs", "tp"),
            P("tp"),
            P(),
            P(),
        ),
        out_specs=P(("rep", "fs"), "tp"),
        check_vma=False,
    )
```

time: 117 us -> 95.8 us (0.82)
  Pallas kernels: 115 us -> 93.8 us
    pallas_call x1, Pallas kernels: 115 us -> 93.8 us  [fused(): pl.pallas_call(functools.partial(kernel, fs, tp), out_shape=jax.ShapeDtyp...]
where the time goes in v2:
time: 95.8 us; the launch traced here: 95.7 us
  Pallas kernels  93.8 us (98%)
  local copies, waits for them, and re-layouts  1.87 us (2%)
    pallas_call x1, Pallas kernels, fused(): pl.pallas_call(functools.partial(kernel, fs, tp), out_shape=jax.ShapeDtyp...  93.8 us

profile of v2, /device:TPU:0, one launch (start us, length us, event | category | flops | bytes accessed | tf_op | source)
XLA Modules:
  0.0 95.7 jit_solution(14575145102273939361)
XLA Ops:
  0.0 93.8 %shard_map.181 = bf16[512,512]{1,0:T(8,128)(2,1)} custom-call(bf16[512,512]{1,0:T(8,128)(2,1)} %tokens_hbm.1, f32[512,128]{1,0:T(8,128)} %outer_hbm.1, f32[512,128]{1,0:T(8,128)} %inner_hbm.1, f32[512,128]{1,0:T(8,128)} %value_hbm.1, f32[128,512]{1,0:T(8,128)} %out_hbm.1, f32[512,768]{1,0:T(8,128)} %up_hbm.1, f32[512,768]{1,0:T(8,128)} %gate_hbm.1, ...), custom_call_target="tpu_custom_call" | custom-call | tf_op jit(solution)/shard_map/pallas_call | solution.py:813
  93.8 1.9 %copy.21 = bf16[512,512]{1,0:T(8,128)(2,1)} copy(bf16[512,512]{1,0:T(8,128)(2,1)} %shard_map.181) | data formatting | bytes 1048576

commit v3 on v2

--- a/solution.py
+++ b/solution.py
@@ -140,8 +140,9 @@
 
 
 LANES = 128
-STAT_ROWS = 8
+STAT_ROWS = 2
 GUEST_PARTS = 2
+ROW_CUT = 128
 RETURN_PARTS = 2
 MIX_PARTS = 4
 BLOCK_PARTS = (1, 1, 1, 1, 1, 2)
@@ -476,10 +477,10 @@
             lines = pl.ds(part * guest_rows, guest_rows)
             send("zi", norm_all.at[t, lines], guest_all.at[t, lines], recv_g.at[part], {"fs": near})
 
-        def units_of(block, left):
-            both = dot32(left(0), ug_g[0, block])
+        def units_of(block, left, lines):
+            both = dot32(left(0, lines), ug_g[0, block])
             for slot in range(1, tp):
-                both = both + dot32(left(slot), ug_g[slot, block])
+                both = both + dot32(left(slot, lines), ug_g[slot, block])
             columns = slice(block * LANES, (block + 1) * LANES)
             mixed = []
             for side in range(2):
@@ -494,12 +495,18 @@
                 )
             return (mixed[0] * mixed[1] / (1.0 + jnp.exp(-mixed[1]))).astype(jnp.bfloat16)
 
+        row_cuts = [slice(first, first + ROW_CUT) for first in range(0, rows, ROW_CUT)]
+
+        def store_units(block, left, target):
+            for lines in row_cuts:
+                target[lines] = units_of(block, lambda slot, lines: left[slot, lines], lines)
+
         def need_block(block):
             for unit in block_units[block]:
                 need(unit)
 
         def hidden(block):
-            hidden_all[t, block] = units_of(block, lambda slot: norm_all[slot])
+            store_units(block, norm_all, hidden_all.at[t, block])
             exchange_start(first_hidden + block * RETURN_PARTS)
 
         def give_back(block):
@@ -511,13 +518,12 @@
                 )
 
         def guest_hidden(block):
-            hidden_out[block] = units_of(block, lambda slot: guest_all[slot])
+            store_units(block, guest_all, hidden_out.at[block])
             give_back(block)
 
         def both_hidden(block):
-            units_both = units_of(block, lambda slot: jnp.concatenate([guest_all[slot], norm_all[slot]], axis=0))
-            hidden_out[block] = units_both[:rows]
-            hidden_all[t, block] = units_both[rows:]
+            store_units(block, guest_all, hidden_out.at[block])
+            store_units(block, norm_all, hidden_all.at[t, block])
             give_back(block)
             exchange_start(first_hidden + block * RETURN_PARTS)
 
@@ -559,209 +565,215 @@
 
         if middle:
             lower_mix()
+            own(3)
             own(0)
+            own(1)
+            own(2)
+            exchange_start(0)
+            from_inner(3, inner, 1)
+            from_outer(2)
+            from_outer(1)
+            from_inner(0, inner, 1)
+            from_outer(0)
+            from_inner(1, inner, 1)
             lower_out()
-            own(2)
-            own(1)
-            exchange_start(0)
-            own(3)
-            from_outer(0)
+            from_outer(3)
+            from_inner(2, inner, 1)
+            from_outer(4)
             lower_down()
-            from_inner(0, inner, 1)
-            from_inner(2, inner, 1)
-            from_outer(2)
-            from_inner(1, inner, 1)
-            from_outer(3)
+            own(4)
+            from_inner(2, far, 2)
             lower_block(3)
-            from_outer(1)
-            own(4)
             from_inner(0, far, 2)
-            lower_block(5)
+            from_inner(1, far, 2)
+            lower_block(1)
+            from_inner(3, far, 2)
+            own(9)
+            exchange_pass(0)
             small_loads()
-            from_inner(3, inner, 1)
-            from_inner(2, far, 2)
-            lower_block(1)
+            lower_block(4)
+            own(11)
+            from_inner(4, inner, 1)
+            lower_block(2)
+            from_inner(4, far, 2)
+            own(5)
             lower_block(0)
-            own(9)
-            from_inner(3, far, 2)
-            from_outer(4)
-            lower_block(4)
-            from_inner(1, far, 2)
-            own(8)
-            exchange_pass(0)
-            own(5)
-            from_inner(4, inner, 1)
             from_inner(9, inner, 1)
             mixer()
-            from_inner(4, far, 2)
+            own(12)
+            own(8)
+            from_inner(11, inner, 1)
+            exchange_pass(1)
+            from_outer(9)
+            from_inner(5, inner, 1)
+            from_outer(7)
+            own(6)
+            from_inner(12, inner, 1)
+            mixer_output()
             from_inner(8, inner, 1)
-            own(11)
+            first_norm()
+            own(10)
+            from_outer(8)
+            exchange_start(2)
+            from_inner(7, far, 2)
+            lower_block(5)
+            from_inner(9, far, 2)
+            from_outer(6)
+            from_inner(6, inner, 1)
+            own(7)
+            from_outer(10)
+            from_outer(5)
+            from_inner(10, inner, 1)
+            guest_start(0)
+            from_inner(6, far, 2)
+            from_inner(8, far, 2)
+            from_inner(7, inner, 1)
+            exchange_pass(2)
+            from_outer(11)
+            guest_start(1)
+            exchange_pass(15)
+            need_block(1)
+            need_block(0)
+            exchange_end(2)
+            from_inner(10, far, 2)
+            exchange_end(15)
+            own(13)
+            from_inner(5, far, 2)
+            hidden(0)
+            from_outer(12)
+            exchange_pass(16)
+            hidden(1)
+            from_outer(13)
             own(14)
-            from_inner(5, inner, 1)
-            own(7)
-            exchange_pass(1)
-            lower_block(2)
-            mixer_output()
-            from_inner(11, inner, 1)
-            from_outer(9)
+            exchange_end(16)
+            from_inner(11, far, 2)
+            guest_hidden(1)
+            guest_hidden(0)
+            from_inner(12, far, 2)
+            from_outer(14)
+            need_block(2)
+            guest_hidden(2)
+            from_inner(13, inner, 1)
+            from_inner(13, far, 2)
             from_inner(14, inner, 1)
-            first_norm()
-            own(12)
-            own(6)
-            exchange_start(2)
-            from_inner(7, inner, 1)
-            from_inner(9, far, 2)
-            from_outer(7)
-            from_inner(12, inner, 1)
-            from_inner(6, inner, 1)
-            from_outer(8)
-            own(10)
-            from_inner(7, far, 2)
-            from_outer(10)
-            guest_start(0)
-            from_outer(6)
-            from_outer(5)
-            exchange_pass(2)
-            from_inner(8, far, 2)
-            from_outer(13)
-            guest_start(1)
-            exchange_end(2)
-            from_inner(10, inner, 1)
-            from_outer(11)
-            exchange_pass(15)
-            from_inner(10, far, 2)
-            from_inner(6, far, 2)
-            exchange_pass(16)
-            from_inner(5, far, 2)
-            from_outer(12)
-            own(13)
-            from_inner(13, far, 2)
-            need_block(0)
-            exchange_end(15)
-            exchange_end(16)
-            need_block(1)
-            both_hidden(1)
-            from_inner(11, far, 2)
-            from_outer(14)
-            both_hidden(0)
-            need_block(2)
-            from_inner(12, far, 2)
-            both_hidden(2)
-            from_inner(13, inner, 1)
             need_block(3)
-            both_hidden(3)
+            hidden(3)
+            guest_hidden(3)
             from_inner(14, far, 2)
+            hidden(2)
+            need_block(4)
+            guest_hidden(4)
+            hidden(4)
+            need_block(5)
+            guest_hidden(5)
+            exchange_pass(7)
+            hidden(5)
+            exchange_pass(3)
             exchange_pass(5)
-            need_block(4)
-            both_hidden(4)
-            need_block(5)
-            both_hidden(5)
+            down(0)
+            exchange_pass(9)
             exchange_pass(11)
-            exchange_pass(7)
-            exchange_pass(3)
-            exchange_pass(9)
             exchange_pass(13)
-            down(0)
             down(1)
             down(2)
             finish()
         else:
             lower_mix()
+            own(2)
+            own(1)
             own(0)
             lower_out()
+            lower_down()
             own(3)
-            own(2)
-            own(1)
+            lower_block(1)
+            exchange_start(0)
             own(4)
-            lower_down()
-            lower_block(3)
+            from_inner(0, near, 0)
             own_rest(3)
-            exchange_start(0)
-            small_loads()
-            from_inner(0, near, 0)
+            from_inner(3, near, 0)
+            own_rest(0)
+            lower_block(5)
             own_rest(1)
+            own_rest(2)
+            from_inner(3, beyond, 1)
             from_inner(2, near, 0)
-            from_inner(3, near, 0)
-            own_rest(2)
-            lower_block(1)
-            own_rest(0)
+            lower_block(4)
+            own(5)
             from_inner(0, beyond, 1)
+            from_inner(1, near, 0)
+            from_inner(1, beyond, 1)
+            from_inner(2, far, 2)
             lower_block(2)
-            own(5)
-            from_inner(2, beyond, 1)
-            own(10)
-            from_inner(1, beyond, 1)
-            lower_block(5)
-            from_inner(1, near, 0)
-            own(9)
-            from_inner(0, far, 2)
-            from_inner(3, beyond, 1)
             own_rest(4)
             lower_block(0)
-            from_inner(2, far, 2)
-            own(6)
-            from_inner(3, far, 2)
+            own(8)
+            own(9)
+            from_inner(2, beyond, 1)
             exchange_pass(0)
             from_inner(1, far, 2)
-            own(11)
+            lower_block(3)
+            from_inner(3, far, 2)
+            own(7)
+            from_inner(0, far, 2)
+            own_rest(8)
+            small_loads()
+            own(6)
+            own(10)
+            from_inner(4, far, 2)
+            from_inner(4, beyond, 1)
             mixer()
             from_inner(4, near, 0)
-            from_inner(4, beyond, 1)
-            from_inner(4, far, 2)
-            own(13)
-            own(7)
+            own(11)
             exchange_pass(1)
-            lower_block(4)
-            own(8)
             mixer_output()
             first_norm()
             guest_send(0)
+            from_inner(7, far, 2)
+            from_inner(5, near, 0)
             guest_send(1)
-            from_inner(5, beyond, 1)
-            from_inner(5, near, 0)
             own_rest(9)
+            own(12)
+            own(13)
+            own_rest(10)
             own(14)
-            from_inner(6, near, 0)
-            own(12)
-            from_inner(7, beyond, 1)
-            own_rest(8)
-            from_inner(7, far, 2)
             own_rest(11)
-            own_rest(10)
-            from_inner(7, near, 0)
-            own_rest(14)
+            from_inner(6, far, 2)
             own_rest(12)
             returned(2)
+            own_rest(14)
+            returned(3)
+            from_inner(6, near, 0)
+            own_rest(13)
+            from_inner(7, beyond, 1)
+            returned(0)
             from_inner(5, far, 2)
-            returned(3)
-            own_rest(13)
-            returned(0)
             returned(1)
-            exchange_pass(6)
+            own_rest(6)
+            own_rest(5)
+            own_rest(7)
             from_inner(6, beyond, 1)
             returned(4)
-            own_rest(6)
             returned(5)
+            exchange_pass(4)
             returned(6)
-            exchange_pass(5)
-            own_rest(5)
-            from_inner(6, far, 2)
-            exchange_pass(4)
-            own_rest(7)
             returned(7)
             returned(8)
+            exchange_pass(6)
+            exchange_pass(8)
+            exchange_pass(5)
             returned(9)
+            from_inner(5, beyond, 1)
+            exchange_pass(10)
+            exchange_pass(9)
+            returned(10)
+            exchange_pass(7)
+            from_inner(7, near, 0)
             exchange_pass(3)
-            returned(10)
-            exchange_pass(10)
-            exchange_pass(8)
-            exchange_pass(7)
+            returned(11)
             exchange_pass(11)
-            returned(11)
-            exchange_pass(9)
+            down(0)
+            exchange_pass(13)
             exchange_pass(12)
-            exchange_pass(13)
-            down(0)
             exchange_pass(14)
             down(1)
             down(2)

time: 95.8 us -> 93.1 us (0.972)
  Pallas kernels: 93.8 us -> 91 us
    pallas_call x1, Pallas kernels: 93.8 us -> 91 us  [fused(): pl.pallas_call(functools.partial(kernel, fs, tp), out_shape=jax.ShapeDtyp...]
where the time goes in v3:
time: 93.1 us; the launch traced here: 92.9 us
  Pallas kernels  91 us (98%)
  local copies, waits for them, and re-layouts  1.87 us (2%)
    pallas_call x1, Pallas kernels, fused(): pl.pallas_call(functools.partial(kernel, fs, tp), out_shape=jax.ShapeDtyp...  91 us
    unnamed x1, local copies, waits for them, and re-layouts  1.87 us

profile of v3, /device:TPU:0, one launch (start us, length us, event | category | flops | bytes accessed | tf_op | source)
XLA Modules:
  0.0 92.9 jit_solution(10296153765247052396)
XLA Ops:
  0.0 91.0 %shard_map.181 = bf16[512,512]{1,0:T(8,128)(2,1)} custom-call(bf16[512,512]{1,0:T(8,128)(2,1)} %tokens_hbm.1, f32[512,128]{1,0:T(8,128)} %outer_hbm.1, f32[512,128]{1,0:T(8,128)} %inner_hbm.1, f32[512,128]{1,0:T(8,128)} %value_hbm.1, f32[128,512]{1,0:T(8,128)} %out_hbm.1, f32[512,768]{1,0:T(8,128)} %up_hbm.1, f32[512,768]{1,0:T(8,128)} %gate_hbm.1, ...), custom_call_target="tpu_custom_call" | custom-call | tf_op jit(solution)/shard_map/pallas_call | solution.py:825
  91.0 1.9 %copy.21 = bf16[512,512]{1,0:T(8,128)(2,1)} copy(bf16[512,512]{1,0:T(8,128)(2,1)} %shard_map.181) | data formatting | bytes 1048576

commit v4 on v3

--- a/solution.py
+++ b/solution.py
@@ -141,7 +141,8 @@
 
 LANES = 128
 STAT_ROWS = 2
-GUEST_PARTS = 2
+GUEST_PARTS = 4
+CONV_PARTS = 2
 ROW_CUT = 128
 RETURN_PARTS = 2
 MIX_PARTS = 4
@@ -219,7 +220,6 @@
     recv_x,
     recv_s,
     recv_g,
-    recv_h,
 ):
     r, z, t = lax.axis_index("rep"), lax.axis_index("fs"), lax.axis_index("tp")
     sibling = t + 1 - 2 * (t % 2)
@@ -241,7 +241,7 @@
     places += (mixer_scales, mixer_taps, out_scale, first_gain, first_shift, up_scales, ffn_taps, ffn_shift)
     places += (down_scale, second_gain, second_shift)
     loads = [
-        pltpu.make_async_copy(source, place, load_sem.at[number])
+        pltpu.make_async_copy(source, place, load_sem.at[max(number - 2, min(number, 1))])
         for number, (source, place) in enumerate(zip(sources, places))
     ]
     for load in loads:
@@ -272,7 +272,9 @@
 
     guest_rows = rows // GUEST_PARTS
     return_rows = rows // RETURN_PARTS
-    first_hidden, first_guest = 3, 3 + blocks * RETURN_PARTS
+    norm_move = 1 + CONV_PARTS
+    first_hidden, first_guest = norm_move + 1, norm_move + 1 + blocks * RETURN_PARTS
+    conv_rows = rows // CONV_PARTS
 
     def offset(value, size):
         return value if isinstance(value, int) else pl.multiple_of(value, size)
@@ -343,8 +345,12 @@
             ).wait_recv()
 
         def moved(number, slot):
-            if number < 3:
-                return (token_all, conv_all, norm_all)[number].at[slot]
+            if number == 0:
+                return token_all.at[slot]
+            if number < norm_move:
+                return conv_all.at[slot, pl.ds((number - 1) * conv_rows, conv_rows)]
+            if number == norm_move:
+                return norm_all.at[slot]
             if number >= first_guest:
                 return guest_all.at[slot, pl.ds((number - first_guest) * guest_rows, guest_rows)]
             block, part = (number - first_hidden) // RETURN_PARTS, (number - first_hidden) % RETURN_PARTS
@@ -394,8 +400,7 @@
             arrived(units[unit](pl.ds(0, 3), 0), gather_sem.at[unit])
 
         def lower_mix():
-            for load in loads[1:4]:
-                load.wait()
+            pltpu.make_async_copy(mix_f, mix_f, load_sem.at[1]).wait()
             for part in range(3):
                 mix_g[z, :, part * channels : (part + 1) * channels] = mix_f[part].astype(jnp.bfloat16)
 
@@ -438,28 +443,31 @@
             average = back[:, 0:1] / full_width
             return average, back[:, 1:2] / full_width - average * average
 
-        def mixer():
-            for unit in range(MIX_PARTS):
-                need(unit)
-            exchange_end(0)
-            gathered = dot32(token_all[0], mix_g[0])
+        def mixer(part):
+            if part == 0:
+                for unit in range(MIX_PARTS):
+                    need(unit)
+                exchange_end(0)
+            lines = slice(part * conv_rows, (part + 1) * conv_rows)
+            gathered = dot32(token_all[0, lines], mix_g[0])
             for slot in range(1, tp):
-                gathered = gathered + dot32(token_all[slot], mix_g[slot])
+                gathered = gathered + dot32(token_all[slot, lines], mix_g[slot])
             scaled = [
-                (gathered[:, part * channels : (part + 1) * channels] * mixer_scales[part : part + 1])
+                (gathered[:, kind * channels : (kind + 1) * channels] * mixer_scales[kind : kind + 1])
                 .astype(jnp.bfloat16)
                 .astype(jnp.float32)
-                for part in range(3)
+                for kind in range(3)
             ]
             mixed = scaled[0] * shifted_mix(
                 scaled[1] * scaled[2], mixer_taps[0:1], mixer_taps[1:2], mixer_taps[2:3]
             )
-            conv_all[t] = mixed.astype(jnp.bfloat16)
-            exchange_start(1)
+            conv_all[t, lines] = mixed.astype(jnp.bfloat16)
+            exchange_start(1 + part)
 
         def mixer_output():
             need(out_index)
-            exchange_end(1)
+            for part in range(CONV_PARTS):
+                exchange_end(1 + part)
             summed = dot32(conv_all[0], out_g[0])
             for slot in range(1, tp):
                 summed = summed + dot32(conv_all[slot], out_g[slot])
@@ -501,6 +509,9 @@
             for lines in row_cuts:
                 target[lines] = units_of(block, lambda slot, lines: left[slot, lines], lines)
 
+        def back_sem(number):
+            return arrive_sem.at[first_ug + number // 3, number % 3]
+
         def need_block(block):
             for unit in block_units[block]:
                 need(unit)
@@ -514,7 +525,7 @@
                 lines = pl.ds(part * return_rows, return_rows)
                 number = block * RETURN_PARTS + part
                 send(
-                    "zo", hidden_out.at[block, lines], hidden_all.at[t, block, lines], recv_h.at[number], {"fs": outer}
+                    "zo", hidden_out.at[block, lines], hidden_all.at[t, block, lines], back_sem(number), {"fs": outer}
                 )
 
         def guest_hidden(block):
@@ -533,7 +544,7 @@
             exchange_start(first_guest + part)
 
         def returned(number):
-            arrived(moved(first_hidden + number, t), recv_h.at[number])
+            arrived(moved(first_hidden + number, t), back_sem(number))
             exchange_start(first_hidden + number)
 
         def hidden_end(block):
@@ -565,216 +576,228 @@
 
         if middle:
             lower_mix()
-            own(3)
-            own(0)
             own(1)
             own(2)
+            lower_out()
             exchange_start(0)
-            from_inner(3, inner, 1)
-            from_outer(2)
-            from_outer(1)
-            from_inner(0, inner, 1)
+            lower_down()
+            own(0)
+            lower_block(2)
+            own(3)
+            lower_block(1)
             from_outer(0)
             from_inner(1, inner, 1)
-            lower_out()
             from_outer(3)
             from_inner(2, inner, 1)
+            from_inner(0, inner, 1)
+            from_outer(1)
+            own(4)
+            from_outer(2)
+            from_inner(3, far, 2)
+            lower_block(4)
             from_outer(4)
-            lower_down()
-            own(4)
+            own(9)
+            from_inner(1, far, 2)
+            from_inner(0, far, 2)
+            from_inner(3, inner, 1)
+            own(12)
             from_inner(2, far, 2)
             lower_block(3)
-            from_inner(0, far, 2)
-            from_inner(1, far, 2)
-            lower_block(1)
-            from_inner(3, far, 2)
-            own(9)
+            from_inner(4, far, 2)
+            small_loads()
+            from_inner(4, inner, 1)
+            lower_block(0)
+            own(5)
             exchange_pass(0)
-            small_loads()
-            lower_block(4)
+            from_outer(7)
+            from_inner(9, inner, 1)
+            mixer(0)
+            mixer(1)
+            own(6)
+            from_outer(9)
+            from_inner(12, inner, 1)
+            exchange_pass(1)
+            own(7)
+            exchange_pass(2)
+            from_inner(5, inner, 1)
+            mixer_output()
+            from_inner(7, far, 2)
+            from_inner(6, inner, 1)
+            from_outer(8)
+            first_norm()
+            exchange_start(3)
+            from_inner(9, far, 2)
+            from_outer(5)
+            lower_block(5)
+            own(8)
+            from_outer(10)
+            from_inner(7, inner, 1)
+            from_inner(8, far, 2)
+            from_inner(5, far, 2)
+            guest_start(2)
+            from_inner(8, inner, 1)
+            from_outer(6)
+            own(10)
+            from_outer(11)
+            guest_start(0)
+            exchange_pass(3)
+            guest_start(1)
+            from_inner(10, far, 2)
+            from_inner(6, far, 2)
             own(11)
-            from_inner(4, inner, 1)
-            lower_block(2)
-            from_inner(4, far, 2)
-            own(5)
-            lower_block(0)
-            from_inner(9, inner, 1)
-            mixer()
-            own(12)
-            own(8)
+            guest_start(3)
+            exchange_pass(16)
+            from_inner(10, inner, 1)
+            exchange_pass(18)
+            exchange_pass(17)
+            from_outer(12)
+            from_outer(14)
+            from_inner(11, far, 2)
+            exchange_pass(19)
+            from_outer(13)
+            exchange_end(3)
+            need_block(0)
             from_inner(11, inner, 1)
-            exchange_pass(1)
-            from_outer(9)
-            from_inner(5, inner, 1)
-            from_outer(7)
-            own(6)
-            from_inner(12, inner, 1)
-            mixer_output()
-            from_inner(8, inner, 1)
-            first_norm()
-            own(10)
-            from_outer(8)
-            exchange_start(2)
-            from_inner(7, far, 2)
-            lower_block(5)
-            from_inner(9, far, 2)
-            from_outer(6)
-            from_inner(6, inner, 1)
-            own(7)
-            from_outer(10)
-            from_outer(5)
-            from_inner(10, inner, 1)
-            guest_start(0)
-            from_inner(6, far, 2)
-            from_inner(8, far, 2)
-            from_inner(7, inner, 1)
-            exchange_pass(2)
-            from_outer(11)
-            guest_start(1)
-            exchange_pass(15)
+            exchange_end(18)
             need_block(1)
-            need_block(0)
-            exchange_end(2)
-            from_inner(10, far, 2)
-            exchange_end(15)
+            exchange_end(16)
+            exchange_end(19)
+            exchange_end(17)
+            guest_hidden(0)
+            hidden(1)
+            own(14)
+            need_block(2)
+            from_inner(12, far, 2)
+            guest_hidden(1)
             own(13)
-            from_inner(5, far, 2)
             hidden(0)
-            from_outer(12)
-            exchange_pass(16)
-            hidden(1)
-            from_outer(13)
-            own(14)
-            exchange_end(16)
-            from_inner(11, far, 2)
-            guest_hidden(1)
-            guest_hidden(0)
-            from_inner(12, far, 2)
-            from_outer(14)
-            need_block(2)
+            from_inner(14, far, 2)
             guest_hidden(2)
+            from_inner(13, far, 2)
+            need_block(3)
+            hidden(2)
+            from_inner(14, inner, 1)
             from_inner(13, inner, 1)
-            from_inner(13, far, 2)
-            from_inner(14, inner, 1)
-            need_block(3)
+            guest_hidden(3)
+            need_block(4)
+            hidden(4)
+            guest_hidden(4)
+            exchange_pass(6)
             hidden(3)
-            guest_hidden(3)
-            from_inner(14, far, 2)
-            hidden(2)
-            need_block(4)
-            guest_hidden(4)
-            hidden(4)
             need_block(5)
+            exchange_pass(4)
             guest_hidden(5)
-            exchange_pass(7)
+            exchange_pass(8)
             hidden(5)
-            exchange_pass(3)
-            exchange_pass(5)
             down(0)
-            exchange_pass(9)
-            exchange_pass(11)
-            exchange_pass(13)
+            exchange_pass(10)
+            exchange_pass(12)
+            exchange_pass(14)
             down(1)
             down(2)
             finish()
         else:
             lower_mix()
-            own(2)
+            own(0)
+            own(3)
+            small_loads()
             own(1)
-            own(0)
             lower_out()
             lower_down()
-            own(3)
+            own(2)
+            own(4)
+            own(7)
+            exchange_start(0)
+            lower_block(0)
+            own_rest(2)
+            from_inner(2, near, 0)
+            from_inner(0, near, 0)
             lower_block(1)
-            exchange_start(0)
-            own(4)
-            from_inner(0, near, 0)
+            from_inner(1, near, 0)
+            lower_block(4)
             own_rest(3)
+            lower_block(5)
+            from_inner(1, beyond, 1)
+            own_rest(1)
+            own_rest(4)
+            own_rest(0)
             from_inner(3, near, 0)
-            own_rest(0)
-            lower_block(5)
-            own_rest(1)
-            own_rest(2)
+            own(9)
+            own(6)
+            from_inner(2, beyond, 1)
+            own(8)
+            from_inner(0, beyond, 1)
+            own(12)
+            from_inner(3, far, 2)
+            from_inner(1, far, 2)
+            from_inner(0, far, 2)
+            exchange_pass(0)
             from_inner(3, beyond, 1)
-            from_inner(2, near, 0)
-            lower_block(4)
             own(5)
-            from_inner(0, beyond, 1)
-            from_inner(1, near, 0)
-            from_inner(1, beyond, 1)
+            lower_block(3)
             from_inner(2, far, 2)
+            from_inner(4, far, 2)
+            mixer(0)
+            mixer(1)
             lower_block(2)
-            own_rest(4)
-            lower_block(0)
-            own(8)
-            own(9)
-            from_inner(2, beyond, 1)
-            exchange_pass(0)
-            from_inner(1, far, 2)
-            lower_block(3)
-            from_inner(3, far, 2)
-            own(7)
-            from_inner(0, far, 2)
-            own_rest(8)
-            small_loads()
-            own(6)
             own(10)
-            from_inner(4, far, 2)
             from_inner(4, beyond, 1)
-            mixer()
             from_inner(4, near, 0)
+            exchange_pass(1)
             own(11)
-            exchange_pass(1)
+            exchange_pass(2)
             mixer_output()
             first_norm()
+            guest_send(2)
             guest_send(0)
-            from_inner(7, far, 2)
+            guest_send(1)
+            own(14)
+            guest_send(3)
+            own(13)
+            own_rest(8)
+            own_rest(9)
+            own_rest(10)
+            own_rest(11)
             from_inner(5, near, 0)
-            guest_send(1)
-            own_rest(9)
-            own(12)
-            own(13)
-            own_rest(10)
-            own(14)
-            own_rest(11)
-            from_inner(6, far, 2)
+            from_inner(5, beyond, 1)
+            from_inner(7, beyond, 1)
             own_rest(12)
+            own_rest(13)
+            returned(0)
+            from_inner(6, near, 0)
+            own_rest(14)
+            from_inner(6, beyond, 1)
+            own_rest(6)
+            returned(1)
             returned(2)
-            own_rest(14)
             returned(3)
-            from_inner(6, near, 0)
-            own_rest(13)
-            from_inner(7, beyond, 1)
-            returned(0)
-            from_inner(5, far, 2)
-            returned(1)
-            own_rest(6)
-            own_rest(5)
-            own_rest(7)
-            from_inner(6, beyond, 1)
             returned(4)
+            from_inner(7, near, 0)
             returned(5)
             exchange_pass(4)
+            from_inner(5, far, 2)
+            own_rest(5)
             returned(6)
+            own_rest(7)
+            from_inner(7, far, 2)
             returned(7)
+            exchange_pass(7)
+            exchange_pass(5)
+            from_inner(6, far, 2)
             returned(8)
+            returned(9)
             exchange_pass(6)
+            returned(10)
+            returned(11)
+            exchange_pass(9)
+            exchange_pass(14)
+            exchange_pass(13)
             exchange_pass(8)
-            exchange_pass(5)
-            returned(9)
-            from_inner(5, beyond, 1)
+            exchange_pass(11)
             exchange_pass(10)
-            exchange_pass(9)
-            returned(10)
-            exchange_pass(7)
-            from_inner(7, near, 0)
-            exchange_pass(3)
-            returned(11)
-            exchange_pass(11)
+            exchange_pass(12)
             down(0)
-            exchange_pass(13)
-            exchange_pass(12)
-            exchange_pass(14)
+            exchange_pass(15)
             down(1)
             down(2)
             finish()
@@ -815,7 +838,7 @@
     hidden = up_proj.shape[1]
     blocks = hidden // LANES
     count = MIX_PARTS + 1 + blocks // 2 + sum(BLOCK_PARTS)
-    moves = 3 + blocks * RETURN_PARTS + GUEST_PARTS
+    moves = 2 + CONV_PARTS + blocks * RETURN_PARTS + GUEST_PARTS
     any_space = pl.BlockSpec(memory_space=pl.ANY)
     in_vmem = pl.BlockSpec(memory_space=pltpu.VMEM)
 
@@ -857,14 +880,13 @@
             pltpu.VMEM((rows, own_width), jnp.float32),
             pltpu.VMEM((rows, own_width), jnp.float32),
             pltpu.VMEM((2, tp, STAT_ROWS, rows), jnp.float32),
-            pltpu.SemaphoreType.DMA((19,)),
+            pltpu.SemaphoreType.DMA((17,)),
             pltpu.SemaphoreType.DMA((sum(LANE_DEPTH.values()),)),
             pltpu.SemaphoreType.DMA((count, 3)),
             pltpu.SemaphoreType.DMA((count,)),
             pltpu.SemaphoreType.DMA((moves, 2)),
             pltpu.SemaphoreType.DMA((2,)),
             pltpu.SemaphoreType.DMA((GUEST_PARTS,)),
-            pltpu.SemaphoreType.DMA((blocks * RETURN_PARTS,)),
         ],
         compiler_params=pltpu.CompilerParams(
             collective_id=0, has_side_effects=True, vmem_limit_bytes=60 * 1024 * 1024

time: 93.1 us -> 91.8 us (0.986)
  Pallas kernels: 91 us -> 89.8 us
    pallas_call x1, Pallas kernels: 91 us -> 89.8 us  [fused(): pl.pallas_call(functools.partial(kernel, fs, tp), out_shape=jax.ShapeDtyp...]
where the time goes in v4:
time: 91.8 us; the launch traced here: 91.7 us
  Pallas kernels  89.8 us (98%)
  local copies, waits for them, and re-layouts  1.87 us (2%)
    pallas_call x1, Pallas kernels, fused(): pl.pallas_call(functools.partial(kernel, fs, tp), out_shape=jax.ShapeDtyp...  89.8 us
    unnamed x1, local copies, waits for them, and re-layouts  1.87 us

profile of v4, /device:TPU:0, one launch (start us, length us, event | category | flops | bytes accessed | tf_op | source)
XLA Modules:
  0.0 91.7 jit_solution(14512983178465217937)
XLA Ops:
  0.0 89.8 %shard_map.181 = bf16[512,512]{1,0:T(8,128)(2,1)} custom-call(bf16[512,512]{1,0:T(8,128)(2,1)} %tokens_hbm.1, f32[512,128]{1,0:T(8,128)} %outer_hbm.1, f32[512,128]{1,0:T(8,128)} %inner_hbm.1, f32[512,128]{1,0:T(8,128)} %value_hbm.1, f32[128,512]{1,0:T(8,128)} %out_hbm.1, f32[512,768]{1,0:T(8,128)} %up_hbm.1, f32[512,768]{1,0:T(8,128)} %gate_hbm.1, ...), custom_call_target="tpu_custom_call" | custom-call | tf_op jit(solution)/shard_map/pallas_call | solution.py:848
  89.8 1.9 %copy.21 = bf16[512,512]{1,0:T(8,128)(2,1)} copy(bf16[512,512]{1,0:T(8,128)(2,1)} %shard_map.181) | data formatting | bytes 1048576

commit v5 on v4

--- a/solution.py
+++ b/solution.py
@@ -143,11 +143,11 @@
 STAT_ROWS = 2
 GUEST_PARTS = 4
 CONV_PARTS = 2
-ROW_CUT = 128
+ROW_CUT = 256
 RETURN_PARTS = 2
 MIX_PARTS = 4
 BLOCK_PARTS = (1, 1, 1, 1, 1, 2)
-LANE_DEPTH = {"zi": 14, "zo": 8, "y": 8, "x": 8, "d": 8}
+LANE_DEPTH = {"zi": 14, "zo": 6, "y": 6, "x": 6, "d": 6}
 
 
 def shifted_mix(signal, first, second, third):

time: 91.8 us -> 91.9 us (level)
  no operation moved by 1% of the time
where the time goes in v5:
time: 91.9 us; the launch traced here: 91.7 us
  Pallas kernels  89.8 us (98%)
  local copies, waits for them, and re-layouts  1.87 us (2%)
    pallas_call x1, Pallas kernels, fused(): pl.pallas_call(functools.partial(kernel, fs, tp), out_shape=jax.ShapeDtyp...  89.8 us
    unnamed x1, local copies, waits for them, and re-layouts  1.87 us

profile of v5, /device:TPU:0, one launch (start us, length us, event | category | flops | bytes accessed | tf_op | source)
XLA Modules:
  0.0 91.7 jit_solution(15185316626983232645)
XLA Ops:
  0.0 89.8 %shard_map.181 = bf16[512,512]{1,0:T(8,128)(2,1)} custom-call(bf16[512,512]{1,0:T(8,128)(2,1)} %tokens_hbm.1, f32[512,128]{1,0:T(8,128)} %outer_hbm.1, f32[512,128]{1,0:T(8,128)} %inner_hbm.1, f32[512,128]{1,0:T(8,128)} %value_hbm.1, f32[128,512]{1,0:T(8,128)} %out_hbm.1, f32[512,768]{1,0:T(8,128)} %up_hbm.1, f32[512,768]{1,0:T(8,128)} %gate_hbm.1, ...), custom_call_target="tpu_custom_call" | custom-call | tf_op jit(solution)/shard_map/pallas_call | solution.py:848
  89.8 1.9 %copy.21 = bf16[512,512]{1,0:T(8,128)(2,1)} copy(bf16[512,512]{1,0:T(8,128)(2,1)} %shard_map.181) | data formatting | bytes 1048576
